TPU v7x, 32 devices: a whole 2x2x4 slice. The times are simulated.
32 devices in a mesh: sp: 4 (over y, x), tp: 8 (over z, core).
Axes of the slice: x: 2, y: 2, z: 4, core: 2. Of those that a mesh axis runs over, the one named last changes fastest.
Arguments:
- lru_input: bfloat16 [1024, 2048], P('sp', 'tp'), may hold values from -27 to 27
- gate_input: bfloat16 [1024, 2048], P('sp', 'tp'), may hold values from -6 to 6
- documents: int32 [1024], P('sp'), may hold values from 0 to 1, never falling along the last dimension, each value on 1 to 768 neighbouring positions
- conv_taps: bfloat16 [4, 2048], P(None, 'tp'), may hold values from -3 to 3
- rate_weight: bfloat16 [16, 128, 128], P('tp'), may hold values from -0.5 to 0.5
- inlet_weight: bfloat16 [16, 128, 128], P('tp'), may hold values from -0.5 to 0.5
- decay_param: float32 [2048], P('tp')
- lru_gain: float32 [2048], P('tp'), may hold values from 0.1 to 1.9
- out_weight: bfloat16 [2048, 2048], P('tp'), may hold values from -0.125 to 0.125
- residual: bfloat16 [1024, 2048], P('sp'), may hold values from -6 to 6
- ffn_gain: float32 [2048], replicated, may hold values from 0.1 to 1.9
- routes: int32 [1024, 2], P('sp'), may hold values from 0 to 3, all different within a row; in each aligned block of 32 rows (0 to 31, 32 to 63, ...) at most 32 rows name the same one
- route_weights: float32 [1024, 2], P('sp'), may hold values from 0.1 to 0.9
- w_gate: bfloat16 [4, 2048, 6144], P('sp', None, 'tp'), may hold values from -0.125 to 0.125
- w_up: bfloat16 [4, 2048, 6144], P('sp', None, 'tp'), may hold values from -0.125 to 0.125
- w_down: bfloat16 [4, 6144, 2048], P('sp', 'tp'), may hold values from -0.078125 to 0.078125
Outputs:
- mixed_out: bfloat16 [1024, 2048], P(('sp', 'tp'))
Inputs may be any that keep to these rules, and one draw needn't show every extreme that they name: `documents`: document numbers start at 0 and never fall along the sequence; a document spans at most 768 positions. `routes`: each row names 2 different experts. In each aligned block of 32 rows no expert is named by more than 32 rows, a bound that some block reaches.
All inputs are finite; a program needn't handle non-finite values.
Results may differ from a plain program's by a relative error of at most 0.017.
Values may be sent and summed in bfloat16 or wider, within the bound.
A program may use at most 64 MiB of HBM per device.

v0:
```python
import functools

import jax
import jax.numpy as jnp
from jax import lax
from jax.experimental import pallas as pl
from jax.experimental.pallas import tpu as pltpu
from jax.sharding import PartitionSpec as P

D_RNN = 2048


EPSILON = 1e-06
RATE_SCALE = 8.0


def shifted(block, axis, distance):
    devices = range(lax.axis_size(axis))
    route = [(i - distance, i) for i in devices if i - distance in devices]
    return lax.ppermute(block, axis, route)


def carried_in(value, axis, join, neutral):
    count, mine = (lax.axis_size(axis), lax.axis_index(axis))
    pieces = jax.tree.map(lambda part: lax.all_gather(part, axis), value)
    so_far = jax.tree.map(
        lambda part, zero: jnp.full_like(part, 0) + jnp.asarray(zero, part.dtype), value, neutral
    )

    def hop(position, so_far):
        longer = join(so_far, jax.tree.map(lambda part: part[position], pieces))
        return jax.tree.map(lambda new, old: jnp.where(position < mine, new, old), longer, so_far)

    return lax.fori_loop(0, count - 1, hop, so_far)


def join_runs(earlier_run, later_run):
    return (earlier_run[0] * later_run[0], later_run[0] * earlier_run[1] + later_run[1])


def slot_targets(route_block, expert_count, capacity):
    flat_routes = route_block.reshape(-1)
    onehot = (flat_routes[:, None] == jnp.arange(expert_count, dtype=jnp.int32)[None, :]).astype(
        jnp.int32
    )
    earlier_hits = jnp.cumsum(onehot, axis=0) - onehot
    slot_index = jnp.sum(earlier_hits * onehot, axis=1)
    return (flat_routes * capacity + slot_index).reshape(route_block.shape)


def pick_matrix(targets, slot_total):
    slot_hits = targets[None, :, :] == jnp.arange(slot_total, dtype=jnp.int32)[:, None, None]
    return jnp.sum(slot_hits.astype(jnp.int32), axis=2).astype(jnp.bfloat16)


def rms_rows(row_block, gain_vector):
    floated = row_block.astype(jnp.float32)
    inverse_rms = lax.rsqrt(jnp.mean(floated * floated, axis=1, keepdims=True) + EPSILON)
    return (floated * inverse_rms * gain_vector[None, :]).astype(jnp.bfloat16)


def expert_apply(row_piece, gate_weight, up_weight, down_weight):
    gate_part = jnp.dot(row_piece, gate_weight, preferred_element_type=jnp.float32)
    up_part = jnp.dot(row_piece, up_weight, preferred_element_type=jnp.float32)
    hidden_units = (jax.nn.silu(gate_part) * up_part).astype(jnp.bfloat16)
    return jnp.dot(hidden_units, down_weight, preferred_element_type=jnp.float32)


def local(
    lru_input,
    gate_input,
    documents,
    conv_taps,
    rate_weight,
    inlet_weight,
    decay_param,
    lru_gain,
    out_weight,
    residual,
    ffn_gain,
    routes,
    route_weights,
    w_gate,
    w_up,
    w_down,
):
    positions = lru_input.shape[0]
    channels = lru_input.shape[1]
    model_width = residual.shape[1]
    reach_back = conv_taps.shape[0] - 1
    tail_rows, tail_docs = shifted(
        (lru_input[positions - reach_back :], documents[positions - reach_back :] + 1), "sp", 1
    )
    prior_docs = jnp.concatenate([tail_docs - 1, documents])
    padded_input = jnp.concatenate([tail_rows, lru_input], axis=0)
    conv_sum = jnp.zeros((positions, channels), jnp.float32)
    for tap_index in range(reach_back + 1):
        same_doc = (prior_docs[tap_index : tap_index + positions] == documents).astype(jnp.float32)[
            :, None
        ]
        conv_sum = (
            conv_sum
            + padded_input[tap_index : tap_index + positions].astype(jnp.float32)
            * conv_taps[tap_index].astype(jnp.float32)[None, :]
            * same_doc
        )
    convolved = conv_sum.astype(jnp.bfloat16)
    grouped = convolved.reshape(positions, rate_weight.shape[0], rate_weight.shape[1])
    rate_gate = jax.nn.sigmoid(
        jnp.einsum(
            "tnc,ncd->tnd", grouped, rate_weight, preferred_element_type=jnp.float32
        ).reshape(positions, channels)
    )
    inlet_gate = jax.nn.sigmoid(
        jnp.einsum(
            "tnc,ncd->tnd", grouped, inlet_weight, preferred_element_type=jnp.float32
        ).reshape(positions, channels)
    )
    log_decay = -RATE_SCALE * rate_gate * jax.nn.softplus(-decay_param)[None, :]
    starts = (prior_docs[reach_back - 1 : reach_back - 1 + positions] != documents)[:, None]
    decay_step = jnp.where(starts, 0.0, jnp.exp(log_decay))
    norm_factor = jnp.where(starts, 1.0, jnp.sqrt(-jnp.expm1(2.0 * log_decay)))
    drive_term = norm_factor * inlet_gate * convolved.astype(jnp.float32)
    decay_run, local_state = lax.associative_scan(join_runs, (decay_step, drive_term), axis=0)
    carried = carried_in(
        (decay_run[positions - 1], local_state[positions - 1]),
        "sp",
        join_runs,
        (jnp.ones((channels,), jnp.float32), jnp.zeros((channels,), jnp.float32)),
    )
    hidden_state = local_state + decay_run * carried[1][None, :]
    square_sums = lax.psum(jnp.sum(hidden_state * hidden_state, axis=1), "tp")
    inverse_rms = lax.rsqrt(square_sums[:, None] / D_RNN + EPSILON)
    mixer_rows = (
        hidden_state * inverse_rms * lru_gain[None, :] * jax.nn.gelu(gate_input.astype(jnp.float32))
    ).astype(jnp.bfloat16)
    tp_count = lax.axis_size("tp")
    tp_here = lax.axis_index("tp")
    expert_count = lax.axis_size("sp")
    route_rows = positions // tp_count
    top_count = routes.shape[1]
    capacity = 2 * top_count * route_rows // expert_count
    slot_total = expert_count * capacity
    projected = lax.psum_scatter(
        jnp.dot(mixer_rows, out_weight, preferred_element_type=jnp.float32).astype(jnp.bfloat16),
        "tp",
        scatter_dimension=0,
        tiled=True,
    ).astype(jnp.float32)
    own_rows = (
        lax.dynamic_slice_in_dim(residual, tp_here * route_rows, route_rows, 0).astype(jnp.float32)
        + projected
    ).astype(jnp.bfloat16)
    own_routes = lax.dynamic_slice_in_dim(routes, tp_here * route_rows, route_rows, 0)
    targets = slot_targets(own_routes, expert_count, capacity)
    outgoing = jnp.dot(
        pick_matrix(targets, slot_total),
        rms_rows(own_rows, ffn_gain),
        preferred_element_type=jnp.float32,
    ).astype(jnp.bfloat16)
    arrived = lax.all_to_all(
        outgoing.reshape(expert_count, capacity, model_width),
        "sp",
        split_axis=0,
        concat_axis=0,
        tiled=True,
    )
    partial_out = expert_apply(
        lax.all_gather(arrived.reshape(slot_total, model_width), "tp", axis=0, tiled=True),
        w_gate[0],
        w_up[0],
        w_down[0],
    )
    expert_out = lax.psum_scatter(
        partial_out.astype(jnp.bfloat16), "tp", scatter_dimension=0, tiled=True
    )
    returned = lax.all_to_all(
        expert_out.reshape(expert_count, capacity, model_width),
        "sp",
        split_axis=0,
        concat_axis=0,
        tiled=True,
    )
    picked = returned.reshape(slot_total, model_width)[targets.reshape(-1)].astype(jnp.float32)
    picked = picked.reshape(route_rows, top_count, model_width)
    own_weights = lax.dynamic_slice_in_dim(route_weights, tp_here * route_rows, route_rows, 0)
    routed = jnp.sum(picked * own_weights[:, :, None], axis=1)
    return (own_rows.astype(jnp.float32) + routed).astype(jnp.bfloat16)


MESH = pl.DeviceIdType.MESH
LANES = 128
GELU_SCALE = 0.7978845608028654


def sender(source, target, send_sem, recv_sem, peer):
    return pltpu.make_async_remote_copy(
        src_ref=source,
        dst_ref=target,
        send_sem=send_sem,
        recv_sem=recv_sem,
        device_id=peer,
        device_id_type=MESH,
    )


def greet(peers):
    barrier = pltpu.get_barrier_semaphore()
    for peer in peers:
        pl.semaphore_signal(barrier, inc=1, device_id=peer, device_id_type=MESH)
    pl.semaphore_wait(barrier, len(peers))


def one_minus_exp(value):
    series = 1.0 + value * (1.0 / 6.0)
    for order in (5.0, 4.0, 3.0, 2.0):
        series = 1.0 + value * (1.0 / order) * series
    return jnp.where(value > -0.25, -value * series, 1.0 - jnp.exp(value))


def down_by(block, distance, filler):
    count = block.shape[0]
    if distance % 8 == 0:
        top = jnp.full((distance, block.shape[1]), filler, block.dtype)
        return jnp.concatenate([top, block[: count - distance]], axis=0)
    row = lax.broadcasted_iota(jnp.int32, block.shape, 0)
    return jnp.where(row >= distance, pltpu.roll(block, distance, 0), filler)


LATE = 8


def layer_kernel(
    n_sp,
    n_tp,
    lru_hbm,
    gate_hbm,
    docs_hbm,
    taps_hbm,
    rate_hbm,
    inlet_hbm,
    decay_hbm,
    gain_hbm,
    out_w_hbm,
    residual_hbm,
    ffn_hbm,
    routes_hbm,
    shares_hbm,
    w_gate_hbm,
    w_up_hbm,
    w_down_hbm,
    out_ref,
    lru_ref,
    gate_ref,
    docs_row,
    taps_ref,
    rate_ref,
    inlet_ref,
    decay_ref,
    gain_ref,
    out_w_ref,
    ffn_ref,
    routes_ref,
    route_w_ref,
    docs_ref,
    weights_ref,
    halo_x,
    halo_d,
    carry_out,
    carry_in,
    share_in,
    run_a,
    run_b,
    parts,
    pair_in,
    z_out,
    z_in,
    squares,
    square_pair,
    square_out,
    square_in,
    res_rows,
    own_ref,
    normed_ref,
    w_gate,
    w_up,
    w_down,
    share_cols,
    blocks,
    hidden_units,
    products,
    back_in,
    joined,
    first_x,
    first_y,
    second_x,
    second_y,
    relay_a,
    relay_b,
    column,
    last_in,
    load_sem,
    res_sem,
    w_sem,
    own_sem,
    halo_s,
    halo_r,
    carry_s,
    carry_r,
    share_s,
    share_r,
    pair_s,
    pair_r,
    z_s,
    z_r,
    gz_s,
    gz_r,
    gxy_s,
    gxy_r,
    gd_s,
    gd_r,
    gp_s,
    gp_r,
    rp_s,
    rp_r,
    r1_s,
    r1_r,
    r2_s,
    r2_r,
    rz_s,
    rz_r,
):
    me_s, me_t = lax.axis_index("sp"), lax.axis_index("tp")
    n_z = n_tp // 2
    me_z, me_c = me_t // 2, me_t % 2
    rows, channels = lru_ref.shape
    width = out_w_ref.shape[1]
    piece = rows // n_tp
    pairs = (
        (lru_hbm, lru_ref),
        (docs_hbm, docs_row),
        (taps_hbm, taps_ref),
        (rate_hbm, rate_ref),
        (inlet_hbm, inlet_ref),
        (decay_hbm, decay_ref),
        (routes_hbm, routes_ref),
        (shares_hbm, route_w_ref),
        (out_w_hbm, out_w_ref),
        (gate_hbm, gate_ref),
        (gain_hbm, gain_ref),
        (ffn_hbm, ffn_ref),
    )
    loads = [
        pltpu.make_async_copy(source, target, load_sem.at[k])
        for k, (source, target) in enumerate(pairs)
    ]
    for copy in loads:
        copy.start()
    residual_copy = pltpu.make_async_copy(
        residual_hbm.at[pl.ds(pl.multiple_of(me_t * piece, piece), piece)], res_rows, res_sem
    )
    residual_copy.start()
    w_loads = [
        pltpu.make_async_copy(source, target, w_sem.at[k])
        for k, (source, target) in enumerate(
            ((w_gate_hbm, w_gate), (w_up_hbm, w_up), (w_down_hbm, w_down))
        )
    ]
    for copy in w_loads:
        copy.start()
    s_x = me_s + 1 - 2 * (me_s % 2)
    s_y = (me_s + 2) % n_sp
    s_d = n_sp - 1 - me_s
    x_peer, y_peer = (s_x, me_t), (s_y, me_t)
    partner = (me_s, me_z * 2 + 1 - me_c)
    sp_peers = [((me_s + k) % n_sp, me_t) for k in range(1, n_sp)]
    across = (me_z, me_z + 1 - 2 * (me_z % 2), n_z - 1 - me_z, (me_z + 2) % n_z)
    z_peers = [(me_s, across[k] * 2 + me_c) for k in range(1, n_z)]
    greet(sp_peers + z_peers + [partner])
    loads[0].wait()
    loads[1].wait()
    docs = jnp.transpose(jnp.broadcast_to(docs_row[...], (8, rows)))
    docs = jnp.broadcast_to(docs[:, :1], (rows, LANES))
    docs_ref[...] = docs
    halo = [
        sender(lru_ref.at[pl.ds(rows - 16, 16)], halo_x, halo_s.at[0], halo_r.at[0], sp_peers[0]),
        sender(docs_ref.at[pl.ds(rows - 8, 8)], halo_d, halo_s.at[1], halo_r.at[1], sp_peers[0]),
    ]
    for copy in halo:
        copy.start()
    loads[6].wait()
    loads[7].wait()
    expert = lax.broadcasted_iota(jnp.int32, weights_ref.shape, 0)
    shares = jnp.zeros(weights_ref.shape, jnp.float32)
    for k in range(routes_ref.shape[0]):
        shares = shares + jnp.where(
            routes_ref[k : k + 1] == expert, route_w_ref[k : k + 1], 0.0
        )
    weights_ref[...] = shares
    share = [
        sender(weights_ref, share_in.at[me_s], share_s.at[k], share_r.at[k], peer)
        for k, peer in enumerate(sp_peers)
    ]
    for copy in share:
        copy.start()
    share_in[pl.ds(me_s, 1)] = shares[None]
    for k in (2, 3, 4, 5, 9, 10, 11):
        loads[k].wait()
    for copy in halo:
        copy.wait()

    before = jnp.where(me_s == 0, jnp.int32(-1), halo_d[...])
    docs_long = jnp.concatenate([before, docs], axis=0)
    taps = taps_ref[...].astype(jnp.float32)
    starts = docs_long[7 : 7 + rows] != docs
    for group in range(channels // LANES):
        span = slice(group * LANES, (group + 1) * LANES)
        long = jnp.concatenate(
            [halo_x[:, span].astype(jnp.float32)[8:], lru_ref[:, span].astype(jnp.float32)], axis=0
        )
        total = jnp.zeros((rows, LANES), jnp.float32)
        for tap in range(taps.shape[0]):
            first = 8 - (taps.shape[0] - 1) + tap
            same = docs_long[first : first + rows] == docs
            total = total + jnp.where(same, long[first : first + rows], 0.0) * taps[tap : tap + 1, span]
        convolved = total.astype(jnp.bfloat16)
        rate = jax.nn.sigmoid(
            jnp.dot(convolved, rate_ref[group], preferred_element_type=jnp.float32)
        )
        inlet = jax.nn.sigmoid(
            jnp.dot(convolved, inlet_ref[group], preferred_element_type=jnp.float32)
        )
        minus = -decay_ref[:, span]
        soft = jnp.maximum(minus, 0.0) + jnp.log1p(jnp.exp(-jnp.abs(minus)))
        log_decay = -RATE_SCALE * rate * soft
        step = jnp.where(starts, 0.0, jnp.exp(log_decay))
        factor = jnp.where(starts, 1.0, jnp.sqrt(one_minus_exp(2.0 * log_decay)))
        state = factor * inlet * convolved.astype(jnp.float32)
        distance = 1
        while distance < rows:
            state = state + step * down_by(state, distance, 0.0)
            step = step * down_by(step, distance, 1.0)
            distance *= 2
        run_a[:, span] = step
        run_b[:, span] = state
        carry_out[:, span] = jnp.concatenate(
            [step[rows - 1 :], state[rows - 1 :], jnp.zeros((6, LANES), jnp.float32)], axis=0
        )
    carry = [
        sender(carry_out, carry_in.at[me_s], carry_s.at[k], carry_r.at[k], peer)
        for k, peer in enumerate(sp_peers)
    ]
    for copy in carry:
        copy.start()
    carry_in[pl.ds(me_s, 1)] = carry_out[...][None]
    raw = gate_ref[...].astype(jnp.float32)
    gelu = 0.5 * raw * (1.0 + jnp.tanh(GELU_SCALE * (raw + 0.044715 * raw * raw * raw)))
    gelu = gelu * gain_ref[...]
    for copy in carry:
        copy.wait()
    carried = jnp.zeros((1, channels), jnp.float32)
    for place in range(n_sp - 1):
        tile = carry_in[place]
        carried = jnp.where(place < me_s, tile[1:2] + tile[0:1] * carried, carried)
    hidden = run_b[...] + run_a[...] * carried
    row_squares = jnp.sum(hidden * hidden, axis=1, keepdims=True)
    squares[...] = jnp.broadcast_to(row_squares, (rows, LANES)).reshape(n_tp, piece, LANES)
    loads[LATE].wait()
    mixer = (hidden * gelu).astype(jnp.bfloat16)
    tile_width = min(512, width)
    for first in range(0, width, tile_width):
        span = slice(first, first + tile_width)
        product = jnp.dot(mixer, out_w_ref[:, span], preferred_element_type=jnp.float32)
        parts[:, :, span] = product.astype(jnp.bfloat16).reshape(n_tp, piece, tile_width)

    order = (across[2], across[3], across[1], me_z)
    pair = []
    for i, z in enumerate(order):
        theirs = z * 2 + 1 - me_c
        pair.append(
            (
                sender(parts.at[theirs], pair_in.at[i], pair_s.at[0, i], pair_r.at[0, i], partner),
                sender(
                    squares.at[theirs], square_pair.at[i], pair_s.at[1, i], pair_r.at[1, i], partner
                ),
            )
        )
        for copy in pair[-1]:
            copy.start()
    z_copies = []
    for i, z in enumerate(order):
        mine = z * 2 + me_c
        for copy in pair[i]:
            copy.wait_recv()
        z_out[i] = (
            parts[mine].astype(jnp.float32) + pair_in[i].astype(jnp.float32)
        ).astype(jnp.bfloat16)
        square_out[i] = squares[mine] + square_pair[i]
        if i < n_z - 1:
            peer = (me_s, mine)
            copies = (
                sender(z_out.at[i], z_in.at[i], z_s.at[0, i], z_r.at[0, i], peer),
                sender(square_out.at[i], square_in.at[i], z_s.at[1, i], z_r.at[1, i], peer),
            )
            for copy in copies:
                copy.start()
            z_copies.append(copies)
    summed = z_out[n_z - 1].astype(jnp.float32)
    square_sum = square_out[n_z - 1]
    for i in range(n_z - 1):
        for copy in z_copies[i]:
            copy.wait_recv()
        summed = summed + z_in[i].astype(jnp.float32)
        square_sum = square_sum + square_in[i]
    inverse = lax.rsqrt(square_sum[:, :1] / (channels * n_tp) + EPSILON)
    residual_copy.wait()
    own = (res_rows[...].astype(jnp.float32) + summed * inverse).astype(jnp.bfloat16)
    own_ref[...] = own
    floated = own.astype(jnp.float32)
    inverse = lax.rsqrt(jnp.mean(floated * floated, axis=1, keepdims=True) + EPSILON)
    normed_ref[...] = (floated * inverse * ffn_ref[...]).astype(jnp.bfloat16)

    half = width // 2
    lower, upper = pl.ds(0, half), pl.ds(half, half)
    sent = []

    def push(source, target, sems, slot, peer):
        copy = sender(source, target, sems[0].at[slot], sems[1].at[slot], peer)
        copy.start()
        sent.append(copy)
        return copy

    gz, gxy, gd, gp = (gz_s, gz_r), (gxy_s, gxy_r), (gd_s, gd_r), (gp_s, gp_r)
    rp, r1, r2, rz = (rp_s, rp_r), (r1_s, r1_r), (r2_s, r2_r), (rz_s, rz_r)
    from_z, from_x, from_y, from_da, from_db, from_pair = {}, {}, {}, {}, {}, {}

    def spread(i):
        block = blocks.at[i, me_s, me_c]
        if i == 0:
            source = normed_ref
        else:
            from_z[i].wait_recv()
            source = block
        from_x[i] = push(source, block, gxy, (0, i), x_peer)
        from_y[i] = push(source, block, gxy, (1, i), y_peer)
        from_pair[0, i] = push(source, block, gp, (0, i), partner)

    def relay(i):
        from_x[i].wait_recv()
        block, part = blocks.at[i, s_x, me_c], blocks.at[i, s_x, me_c, :, lower]
        from_da[i] = push(part, part, gd, (0, i), y_peer)
        from_pair[1, i] = push(block, block, gp, (1, i), partner)
        from_y[i].wait_recv()
        block, part = blocks.at[i, s_y, me_c], blocks.at[i, s_y, me_c, :, upper]
        from_db[i] = push(part, part, gd, (1, i), x_peer)
        from_pair[2, i] = push(block, block, gp, (2, i), partner)

    def hand_over(i):
        from_da[i].wait_recv()
        part = blocks.at[i, s_d, me_c, :, lower]
        from_pair[3, i] = push(part, part, gp, (3, i), partner)
        from_db[i].wait_recv()
        part = blocks.at[i, s_d, me_c, :, upper]
        from_pair[4, i] = push(part, part, gp, (4, i), partner)

    own_copy = pltpu.make_async_copy(normed_ref, blocks.at[0, me_s, me_c], own_sem)
    own_copy.start()
    spread(0)
    for k in range(n_z - 1):
        from_z[k + 1] = push(normed_ref, blocks.at[k + 1, me_s, me_c], gz, k, z_peers[k])
    for copy in share:
        copy.wait()
    for place in range(n_sp):
        turned = jnp.transpose(share_in[place])
        lane = lax.broadcasted_iota(jnp.int32, turned.shape, 1)
        chosen = jnp.sum(jnp.where(lane == me_s, turned, 0.0), axis=1, keepdims=True)
        share_cols[place] = jnp.broadcast_to(chosen, (rows, LANES))

    ff = w_gate.shape[1]
    f_tile, d_tile = 256, min(512, width)
    count = n_sp * 2 * piece
    back, first_xs, first_ys, second_xs, second_ys, back_z = {}, {}, {}, {}, {}, {}

    def rise(i):
        for k in range(5):
            from_pair[k, i].wait_recv()
        tokens = blocks[i].reshape(count, width)

        def up_step(step, _):
            span = pl.ds(pl.multiple_of(step * f_tile, f_tile), f_tile)
            gate_part = jnp.dot(tokens, w_gate[:, span], preferred_element_type=jnp.float32)
            up_part = jnp.dot(tokens, w_up[:, span], preferred_element_type=jnp.float32)
            hidden_units[:, span] = (gate_part * jax.nn.sigmoid(gate_part) * up_part).astype(
                jnp.bfloat16
            )
            return 0

        lax.fori_loop(0, ff // f_tile, up_step, 0)

    def fall(i):
        z = across[i]
        first = pl.multiple_of(z * (2 * piece), 2 * piece)
        scale = share_cols[:, pl.ds(first, 2 * piece), :].reshape(count, LANES)[:, :1]
        units = hidden_units[...]

        def down_step(step, _):
            span = pl.ds(pl.multiple_of(step * d_tile, d_tile), d_tile)
            product = jnp.dot(units, w_down[:, span], preferred_element_type=jnp.float32) * scale
            products[i, :, :, :, span] = product.astype(jnp.bfloat16).reshape(
                n_sp, 2, piece, d_tile
            )
            return 0

        lax.fori_loop(0, width // d_tile, down_step, 0)
        for k, group in enumerate((s_d, s_x, s_y, me_s)):
            back[k, i] = push(
                products.at[i, group, 1 - me_c], back_in.at[i, k], rp, (k, i), partner
            )

    def join(i):
        for k, group in enumerate((s_d, s_x, s_y, me_s)):
            back[k, i].wait_recv()
            joined[i, k] = (
                products[i, group, me_c].astype(jnp.float32) + back_in[i, k].astype(jnp.float32)
            ).astype(jnp.bfloat16)
            if k == 0:
                first_xs[1, i] = push(
                    joined.at[i, 0, :, lower], first_x.at[1, i], r1, (2, i), x_peer
                )
                first_ys[1, i] = push(
                    joined.at[i, 0, :, upper], first_y.at[1, i], r1, (3, i), y_peer
                )
            elif k == 1:
                first_xs[0, i] = push(
                    joined.at[i, 1, :, lower], first_x.at[0, i], r1, (0, i), x_peer
                )
            elif k == 2:
                first_ys[0, i] = push(
                    joined.at[i, 2, :, upper], first_y.at[0, i], r1, (1, i), y_peer
                )

    def turn(i):
        first_xs[1, i].wait_recv()
        relay_a[i] = (
            joined[i, 2, :, :half].astype(jnp.float32) + first_x[1, i].astype(jnp.float32)
        ).astype(jnp.bfloat16)
        second_ys[i] = push(relay_a.at[i], second_y.at[i], r2, (0, i), y_peer)
        first_ys[1, i].wait_recv()
        relay_b[i] = (
            joined[i, 1, :, half:].astype(jnp.float32) + first_y[1, i].astype(jnp.float32)
        ).astype(jnp.bfloat16)
        second_xs[i] = push(relay_b.at[i], second_x.at[i], r2, (1, i), x_peer)

    def finish(i):
        for copies in (first_xs, first_ys):
            copies[0, i].wait_recv()
        for copies in (second_xs, second_ys):
            copies[i].wait_recv()
        low = (
            joined[i, 3, :, :half].astype(jnp.float32)
            + first_x[0, i].astype(jnp.float32)
            + second_y[i].astype(jnp.float32)
        )
        high = (
            joined[i, 3, :, half:].astype(jnp.float32)
            + first_y[0, i].astype(jnp.float32)
            + second_x[i].astype(jnp.float32)
        )
        column[i] = jnp.concatenate([low, high], axis=1).astype(jnp.bfloat16)
        if i > 0:
            peer = z_peers[i - 1]
            back_z[i] = push(column.at[i], last_in.at[i], rz, i, peer)

    own_copy.wait()
    for copy in w_loads:
        copy.wait()
    last = n_z - 1
    spread(1)
    for tick in range(-2, n_z + 2):
        plan = (
            (relay, tick + 2),
            (spread, tick + 3),
            (hand_over, tick + 1),
            (rise, tick),
            (join, tick - 1),
            (finish, tick - 2),
            (fall, tick),
            (turn, tick - 1),
        )
        for stage, i in plan:
            if 0 <= i <= last and not (stage is spread and i <= 1):
                stage(i)
    total = own_ref[...].astype(jnp.float32) + column[0].astype(jnp.float32)
    for i in range(1, n_z):
        back_z[i].wait_recv()
        total = total + last_in[i].astype(jnp.float32)
    out_ref[...] = total.astype(jnp.bfloat16)
    for copies in pair + z_copies:
        for copy in copies:
            copy.wait_send()
    for copy in sent:
        copy.wait_send()


def dense_local(
    lru_input,
    gate_input,
    documents,
    conv_taps,
    rate_weight,
    inlet_weight,
    decay_param,
    lru_gain,
    out_weight,
    residual,
    ffn_gain,
    routes,
    route_weights,
    w_gate,
    w_up,
    w_down,
):
    n_sp, n_tp = lax.axis_size("sp"), lax.axis_size("tp")
    n_z = n_tp // 2
    rows, channels = lru_input.shape
    width = residual.shape[1]
    ff = w_gate.shape[2]
    piece = rows // n_tp
    padded = -(-n_sp // 8) * 8
    vmem = pl.BlockSpec(memory_space=pltpu.VMEM)
    half = width // 2
    top = routes.shape[1]
    hbm = pl.BlockSpec(memory_space=pl.ANY)
    bf16, f32 = jnp.bfloat16, jnp.float32
    dma = pltpu.SemaphoreType.DMA
    rows_buffer = pltpu.VMEM((n_z, piece, width), bf16)
    half_buffer = pltpu.VMEM((n_z, piece, half), bf16)
    chunks = pltpu.VMEM((n_z, n_sp, 2, piece, width), bf16)
    groups = pltpu.VMEM((n_z, n_sp, piece, width), bf16)
    square_buffer = pltpu.VMEM((n_z, piece, LANES), f32)
    shapes = (
        [(2,)] * 2
        + [(n_sp,)] * 4
        + [(2, n_z)] * 4
        + [(n_z,)] * 2
        + [(2, n_z)] * 4
        + [(5, n_z)] * 2
        + [(4, n_z)] * 4
        + [(2, n_z)] * 2
        + [(n_z,)] * 2
    )
    return pl.pallas_call(
        functools.partial(layer_kernel, n_sp, n_tp),
        out_shape=jax.ShapeDtypeStruct((piece, width), bf16),
        in_specs=[hbm] * 16,
        out_specs=vmem,
        scratch_shapes=[
            pltpu.VMEM((rows, channels), bf16),
            pltpu.VMEM((rows, channels), bf16),
            pltpu.VMEM((1, rows), jnp.int32),
            pltpu.VMEM(conv_taps.shape, bf16),
            pltpu.VMEM(rate_weight.shape, bf16),
            pltpu.VMEM(inlet_weight.shape, bf16),
            pltpu.VMEM((1, channels), f32),
            pltpu.VMEM((1, channels), f32),
            pltpu.VMEM((channels, width), bf16),
            pltpu.VMEM((1, width), f32),
            pltpu.VMEM((top, rows), jnp.int32),
            pltpu.VMEM((top, rows), f32),
            pltpu.VMEM((rows, LANES), jnp.int32),
            pltpu.VMEM((padded, rows), f32),
            pltpu.VMEM((16, channels), bf16),
            pltpu.VMEM((8, LANES), jnp.int32),
            pltpu.VMEM((8, channels), f32),
            pltpu.VMEM((n_sp, 8, channels), f32),
            pltpu.VMEM((n_sp, padded, rows), f32),
            pltpu.VMEM((rows, channels), f32),
            pltpu.VMEM((rows, channels), f32),
            pltpu.VMEM((n_tp, piece, width), bf16),
            rows_buffer,
            rows_buffer,
            rows_buffer,
            pltpu.VMEM((n_tp, piece, LANES), f32),
            square_buffer,
            square_buffer,
            square_buffer,
            pltpu.VMEM((piece, width), bf16),
            pltpu.VMEM((piece, width), bf16),
            pltpu.VMEM((piece, width), bf16),
            pltpu.VMEM((width, ff), bf16),
            pltpu.VMEM((width, ff), bf16),
            pltpu.VMEM((ff, width), bf16),
            pltpu.VMEM((n_sp, rows, LANES), f32),
            chunks,
            pltpu.VMEM((n_sp * 2 * piece, ff), bf16),
            chunks,
            groups,
            groups,
            pltpu.VMEM((2, n_z, piece, half), bf16),
            pltpu.VMEM((2, n_z, piece, half), bf16),
            half_buffer,
            half_buffer,
            half_buffer,
            half_buffer,
            rows_buffer,
            rows_buffer,
            dma((12,)),
            dma,
            dma((3,)),
            dma,
        ]
        + [dma(shape) for shape in shapes],
        compiler_params=pltpu.CompilerParams(
            collective_id=0, has_side_effects=True, vmem_limit_bytes=60 * 2**20
        ),
    )(
        lru_input,
        gate_input,
        documents[None, :],
        conv_taps,
        rate_weight,
        inlet_weight,
        decay_param[None, :],
        lru_gain[None, :],
        out_weight,
        residual,
        ffn_gain[None, :],
        routes.T,
        route_weights.T,
        w_gate[0],
        w_up[0],
        w_down[0],
    )


def solution(mesh):
    n_sp, n_tp = mesh.shape["sp"], mesh.shape["tp"]
    body = dense_local if n_sp == 4 and n_tp == 8 else local
    return jax.shard_map(
        body,
        mesh=mesh,
        in_specs=(
            P("sp", "tp"),
            P("sp", "tp"),
            P("sp"),
            P(None, "tp"),
            P("tp", None, None),
            P("tp", None, None),
            P("tp"),
            P("tp"),
            P("tp", None),
            P("sp", None),
            P(),
            P("sp", None),
            P("sp", None),
            P("sp", None, "tp"),
            P("sp", None, "tp"),
            P("sp", "tp", None),
        ),
        out_specs=P(("sp", "tp"), None),
        check_vma=False,
    )
```

profile of v0, /device:TPU:0, one launch (start us, length us, event | category | flops | bytes accessed | tf_op | source)
XLA Modules:
  0.0 86.9 jit_solution(9797392077727853140)
XLA Ops:
  0.0 85.4 %shard_map.154 = bf16[32,2048]{1,0:T(8,128)(2,1)} custom-call(bf16[256,256]{1,0:T(8,128)(2,1)} %lru_hbm.1, bf16[256,256]{1,0:T(8,128)(2,1)} %gate_hbm.1, s32[1,256]{1,0:T(1,128)} %bitcast.15, bf16[4,256]{1,0:T(4,128)(2,1)} %taps_hbm.1, bf16[2,128,128]{2,1,0:T(8,128)(2,1)} %rate_hbm.1, bf16[2,128,128]{2,1,0:T(8,128)(2,1)} %inlet_hbm.1, f32[1,256]{1,0:T(1,128)} %bitcast.16, ...), custom_call_target="tpu_custom_call" | custom-call | tf_op jit(solution)/shard_map/pallas_call | solution.py:752
  85.4 1.6 %copy.18 = bf16[32,2048]{1,0:T(8,128)(2,1)} copy(bf16[32,2048]{1,0:T(8,128)(2,1)} %shard_map.154) | data formatting | bytes 262144
where the time goes:
time: 87.1 us; the launch traced here: 86.9 us
  Pallas kernels  85.4 us (98%)
  local copies, waits for them, and re-layouts  1.57 us (2%)
    pallas_call x1, Pallas kernels, dense_local(): pl.pallas_call(functools.partial(layer_kernel, n_sp, n_tp), out_shape=jax...  85.4 us

commit v1 on v0

--- a/solution.py
+++ b/solution.py
@@ -264,10 +264,14 @@
     route_w_ref,
     docs_ref,
     weights_ref,
-    halo_x,
-    halo_d,
+    edge_out,
+    edge_in,
+    mark_out,
+    mark_in,
     carry_out,
     carry_in,
+    head_a,
+    head_b,
     share_in,
     run_a,
     run_b,
@@ -275,6 +279,8 @@
     pair_in,
     z_out,
     z_in,
+    z_sum,
+    z_across,
     squares,
     square_pair,
     square_out,
@@ -303,8 +309,10 @@
     res_sem,
     w_sem,
     own_sem,
-    halo_s,
-    halo_r,
+    edge_s,
+    edge_r,
+    mark_s,
+    mark_r,
     carry_s,
     carry_r,
     share_s,
@@ -313,6 +321,8 @@
     pair_r,
     z_s,
     z_r,
+    sq_s,
+    sq_r,
     gz_s,
     gz_r,
     gxy_s,
@@ -366,28 +376,86 @@
             ((w_gate_hbm, w_gate), (w_up_hbm, w_up), (w_down_hbm, w_down))
         )
     ]
-    for copy in w_loads:
-        copy.start()
     s_x = me_s + 1 - 2 * (me_s % 2)
     s_y = (me_s + 2) % n_sp
     s_d = n_sp - 1 - me_s
     x_peer, y_peer = (s_x, me_t), (s_y, me_t)
     partner = (me_s, me_z * 2 + 1 - me_c)
     sp_peers = [((me_s + k) % n_sp, me_t) for k in range(1, n_sp)]
-    across = (me_z, me_z + 1 - 2 * (me_z % 2), n_z - 1 - me_z, (me_z + 2) % n_z)
+    z_near, z_far = me_z + 1 - 2 * (me_z % 2), n_z - 1 - me_z
+    upper_side = me_z // 2
+    across = (me_z, z_near, 2 - upper_side, 3 - 3 * upper_side)
+    middle = (me_z + 1) // 2 % 2 == 1
+    outer = (me_z + 1) // 2 % 2 == 0
+    near, over = (me_s, z_near * 2 + me_c), (me_s, z_far * 2 + me_c)
     z_peers = [(me_s, across[k] * 2 + me_c) for k in range(1, n_z)]
-    greet(sp_peers + z_peers + [partner])
-    loads[0].wait()
-    loads[1].wait()
+    greeted = sp_peers + z_peers + [partner]
+    barrier = pltpu.get_barrier_semaphore()
+    for peer in greeted:
+        pl.semaphore_signal(barrier, inc=1, device_id=peer, device_id_type=MESH)
+    for k in range(6):
+        loads[k].wait()
+    for copy in w_loads:
+        copy.start()
     docs = jnp.transpose(jnp.broadcast_to(docs_row[...], (8, rows)))
     docs = jnp.broadcast_to(docs[:, :1], (rows, LANES))
     docs_ref[...] = docs
-    halo = [
-        sender(lru_ref.at[pl.ds(rows - 16, 16)], halo_x, halo_s.at[0], halo_r.at[0], sp_peers[0]),
-        sender(docs_ref.at[pl.ds(rows - 8, 8)], halo_d, halo_s.at[1], halo_r.at[1], sp_peers[0]),
-    ]
-    for copy in halo:
+    lane8 = lax.broadcasted_iota(jnp.int32, (8, LANES), 1)
+    mark_out[...] = jnp.where(lane8 == 0, docs[:8], docs[rows - 8 :])
+    edge_out[0:16] = lru_ref[0:16]
+    edge_out[16:32] = lru_ref[rows - 16 :]
+    taps = taps_ref[...].astype(jnp.float32)
+    reach = taps.shape[0] - 1
+
+    def gates(convolved, starts, group):
+        span = slice(group * LANES, (group + 1) * LANES)
+        rate = jax.nn.sigmoid(
+            jnp.dot(convolved, rate_ref[group], preferred_element_type=jnp.float32)
+        )
+        inlet = jax.nn.sigmoid(
+            jnp.dot(convolved, inlet_ref[group], preferred_element_type=jnp.float32)
+        )
+        minus = -decay_ref[:, span]
+        soft = jnp.maximum(minus, 0.0) + jnp.log1p(jnp.exp(-jnp.abs(minus)))
+        log_decay = -RATE_SCALE * rate * soft
+        step = jnp.where(starts, 0.0, jnp.exp(log_decay))
+        factor = jnp.where(starts, 1.0, jnp.sqrt(one_minus_exp(2.0 * log_decay)))
+        return step, factor * inlet * convolved.astype(jnp.float32)
+
+    body = rows - 8
+    starts = docs[7 : 7 + body] != docs[8:]
+    for group in range(channels // LANES):
+        span = slice(group * LANES, (group + 1) * LANES)
+        long = lru_ref[:, span].astype(jnp.float32)
+        total = jnp.zeros((body, LANES), jnp.float32)
+        for tap in range(reach + 1):
+            first = 8 - reach + tap
+            same = docs[first : first + body] == docs[8:]
+            total = total + jnp.where(same, long[first : first + body], 0.0) * taps[tap : tap + 1, span]
+        step, state = gates(total.astype(jnp.bfloat16), starts, group)
+        distance = 1
+        while distance < body:
+            state = state + step * down_by(state, distance, 0.0)
+            step = step * down_by(step, distance, 1.0)
+            distance *= 2
+        run_a[8:, span] = step
+        run_b[8:, span] = state
+        carry_out[:, span] = jnp.concatenate(
+            [step[body - 1 :], state[body - 1 :], jnp.zeros((6, LANES), jnp.float32)], axis=0
+        )
+    pl.semaphore_wait(barrier, len(greeted))
+    carry = []
+    for k, peer in enumerate(sp_peers):
+        carry += [
+            sender(carry_out, carry_in.at[me_s], carry_s.at[k], carry_r.at[k], peer),
+            sender(mark_out, mark_in.at[me_s], mark_s.at[k], mark_r.at[k], peer),
+            sender(edge_out, edge_in.at[me_s], edge_s.at[k], edge_r.at[k], peer),
+        ]
+    for copy in carry:
         copy.start()
+    carry_in[pl.ds(me_s, 1)] = carry_out[...][None]
+    mark_in[pl.ds(me_s, 1)] = mark_out[...][None]
+    edge_in[pl.ds(me_s, 1)] = edge_out[...][None]
     loads[6].wait()
     loads[7].wait()
     expert = lax.broadcasted_iota(jnp.int32, weights_ref.shape, 0)
@@ -404,67 +472,67 @@
     for copy in share:
         copy.start()
     share_in[pl.ds(me_s, 1)] = shares[None]
-    for k in (2, 3, 4, 5, 9, 10, 11):
+    for k in (9, 10, 11):
         loads[k].wait()
-    for copy in halo:
-        copy.wait()
-
-    before = jnp.where(me_s == 0, jnp.int32(-1), halo_d[...])
-    docs_long = jnp.concatenate([before, docs], axis=0)
-    taps = taps_ref[...].astype(jnp.float32)
-    starts = docs_long[7 : 7 + rows] != docs
-    for group in range(channels // LANES):
-        span = slice(group * LANES, (group + 1) * LANES)
-        long = jnp.concatenate(
-            [halo_x[:, span].astype(jnp.float32)[8:], lru_ref[:, span].astype(jnp.float32)], axis=0
-        )
-        total = jnp.zeros((rows, LANES), jnp.float32)
-        for tap in range(taps.shape[0]):
-            first = 8 - (taps.shape[0] - 1) + tap
-            same = docs_long[first : first + rows] == docs
-            total = total + jnp.where(same, long[first : first + rows], 0.0) * taps[tap : tap + 1, span]
-        convolved = total.astype(jnp.bfloat16)
-        rate = jax.nn.sigmoid(
-            jnp.dot(convolved, rate_ref[group], preferred_element_type=jnp.float32)
-        )
-        inlet = jax.nn.sigmoid(
-            jnp.dot(convolved, inlet_ref[group], preferred_element_type=jnp.float32)
-        )
-        minus = -decay_ref[:, span]
-        soft = jnp.maximum(minus, 0.0) + jnp.log1p(jnp.exp(-jnp.abs(minus)))
-        log_decay = -RATE_SCALE * rate * soft
-        step = jnp.where(starts, 0.0, jnp.exp(log_decay))
-        factor = jnp.where(starts, 1.0, jnp.sqrt(one_minus_exp(2.0 * log_decay)))
-        state = factor * inlet * convolved.astype(jnp.float32)
-        distance = 1
-        while distance < rows:
-            state = state + step * down_by(state, distance, 0.0)
-            step = step * down_by(step, distance, 1.0)
-            distance *= 2
-        run_a[:, span] = step
-        run_b[:, span] = state
-        carry_out[:, span] = jnp.concatenate(
-            [step[rows - 1 :], state[rows - 1 :], jnp.zeros((6, LANES), jnp.float32)], axis=0
-        )
-    carry = [
-        sender(carry_out, carry_in.at[me_s], carry_s.at[k], carry_r.at[k], peer)
-        for k, peer in enumerate(sp_peers)
-    ]
-    for copy in carry:
-        copy.start()
-    carry_in[pl.ds(me_s, 1)] = carry_out[...][None]
     raw = gate_ref[...].astype(jnp.float32)
     gelu = 0.5 * raw * (1.0 + jnp.tanh(GELU_SCALE * (raw + 0.044715 * raw * raw * raw)))
     gelu = gelu * gain_ref[...]
     for copy in carry:
         copy.wait()
+    xs, now, prior = [], [], []
+    for place in range(n_sp):
+        marks = mark_in[place]
+        now.append(jnp.broadcast_to(marks[:, 0:1], (8, LANES)))
+        if place == 0:
+            prior.append(jnp.full((8, LANES), -1, jnp.int32))
+        else:
+            prior.append(jnp.broadcast_to(mark_in[place - 1][:, 1:2], (8, LANES)))
+        xs.append(
+            jnp.concatenate(
+                [
+                    edge_in[max(place - 1, 0)].astype(jnp.float32)[24:],
+                    edge_in[place].astype(jnp.float32)[:8],
+                ],
+                axis=0,
+            )
+        )
+    both = [jnp.concatenate([prior[p], now[p]], axis=0) for p in range(n_sp)]
+    head_starts = jnp.concatenate([both[p][7:15] != now[p] for p in range(n_sp)], axis=0)
+    in_tile = lax.broadcasted_iota(jnp.int32, (8 * n_sp, LANES), 0) % 8
+    for group in range(channels // LANES):
+        span = slice(group * LANES, (group + 1) * LANES)
+        sums = []
+        for place in range(n_sp):
+            total = jnp.zeros((8, LANES), jnp.float32)
+            for tap in range(reach + 1):
+                first = 8 - reach + tap
+                same = both[place][first : first + 8] == now[place]
+                total = total + (
+                    jnp.where(same, xs[place][first : first + 8, span], 0.0)
+                    * taps[tap : tap + 1, span]
+                )
+            sums.append(total)
+        step, state = gates(jnp.concatenate(sums, axis=0).astype(jnp.bfloat16), head_starts, group)
+        for distance in (1, 2, 4):
+            inside = in_tile >= distance
+            state = state + step * jnp.where(inside, pltpu.roll(state, distance, 0), 0.0)
+            step = step * jnp.where(inside, pltpu.roll(step, distance, 0), 1.0)
+        head_a[:, :, span] = step.reshape(n_sp, 8, LANES)
+        head_b[:, :, span] = state.reshape(n_sp, 8, LANES)
     carried = jnp.zeros((1, channels), jnp.float32)
     for place in range(n_sp - 1):
+        entered = head_b[place][7:] + head_a[place][7:] * carried
         tile = carry_in[place]
-        carried = jnp.where(place < me_s, tile[1:2] + tile[0:1] * carried, carried)
-    hidden = run_b[...] + run_a[...] * carried
+        carried = jnp.where(place < me_s, tile[1:2] + tile[0:1] * entered, carried)
+    top = head_b[pl.ds(me_s, 1)][0] + head_a[pl.ds(me_s, 1)][0] * carried
+    hidden = jnp.concatenate([top, run_b[8:] + run_a[8:] * top[7:]], axis=0)
     row_squares = jnp.sum(hidden * hidden, axis=1, keepdims=True)
-    squares[...] = jnp.broadcast_to(row_squares, (rows, LANES)).reshape(n_tp, piece, LANES)
+    for place in range(n_tp):
+        packed = jnp.zeros((8, LANES), jnp.float32)
+        for j in range(piece // 8):
+            first = place * piece + j * 8
+            packed = jnp.where(lane8 == j, row_squares[first : first + 8], packed)
+        squares[place] = packed
     loads[LATE].wait()
     mixer = (hidden * gelu).astype(jnp.bfloat16)
     tile_width = min(512, width)
@@ -473,46 +541,105 @@
         product = jnp.dot(mixer, out_w_ref[:, span], preferred_element_type=jnp.float32)
         parts[:, :, span] = product.astype(jnp.bfloat16).reshape(n_tp, piece, tile_width)
 
-    order = (across[2], across[3], across[1], me_z)
+    half = width // 2
+    halves = (pl.ds(0, half), pl.ds(half, half))
     pair = []
-    for i, z in enumerate(order):
-        theirs = z * 2 + 1 - me_c
+    for i in (3, 2, 1, 0):
+        theirs = across[i] * 2 + 1 - me_c
         pair.append(
             (
+                sender(squares.at[theirs], square_pair.at[i], pair_s.at[1, i], pair_r.at[1, i], partner),
                 sender(parts.at[theirs], pair_in.at[i], pair_s.at[0, i], pair_r.at[0, i], partner),
-                sender(
-                    squares.at[theirs], square_pair.at[i], pair_s.at[1, i], pair_r.at[1, i], partner
-                ),
             )
         )
         for copy in pair[-1]:
             copy.start()
-    z_copies = []
-    for i, z in enumerate(order):
-        mine = z * 2 + me_c
-        for copy in pair[i]:
+    square_copies = []
+    inward = {}
+    for i in (3, 2, 1):
+        for h in range(2):
+            inward[i, h] = sender(
+                z_out.at[i, :, halves[h]], z_in.at[i, :, halves[h]], z_s.at[h, i], z_r.at[h, i], near
+            )
+    for n, i in enumerate((3, 2, 1, 0)):
+        mine = across[i] * 2 + me_c
+        for copy in pair[n]:
             copy.wait_recv()
+        square_out[i] = squares[mine] + square_pair[i]
+        if i > 0:
+            copy = sender(
+                square_out.at[i], square_in.at[me_z], sq_s.at[i], sq_r.at[me_z], z_peers[i - 1]
+            )
+            copy.start()
+            square_copies.append(copy)
         z_out[i] = (
             parts[mine].astype(jnp.float32) + pair_in[i].astype(jnp.float32)
         ).astype(jnp.bfloat16)
-        square_out[i] = squares[mine] + square_pair[i]
-        if i < n_z - 1:
-            peer = (me_s, mine)
-            copies = (
-                sender(z_out.at[i], z_in.at[i], z_s.at[0, i], z_r.at[0, i], peer),
-                sender(square_out.at[i], square_in.at[i], z_s.at[1, i], z_r.at[1, i], peer),
+
+        if i > 0:
+
+            @pl.when(outer)
+            def _():
+                for h in range(2):
+                    inward[i, h].start()
+
+    crossing, outward = {}, {}
+    for i in (3, 2):
+        for h in range(2):
+            crossing[i, h] = sender(
+                z_sum.at[i, :, halves[h]], z_across.at[i, :, halves[h]], z_s.at[h, i + 2], z_r.at[h, i + 2], over
             )
-            for copy in copies:
-                copy.start()
-            z_copies.append(copies)
-    summed = z_out[n_z - 1].astype(jnp.float32)
-    square_sum = square_out[n_z - 1]
-    for i in range(n_z - 1):
-        for copy in z_copies[i]:
-            copy.wait_recv()
-        summed = summed + z_in[i].astype(jnp.float32)
-        square_sum = square_sum + square_in[i]
-    inverse = lax.rsqrt(square_sum[:, :1] / (channels * n_tp) + EPSILON)
+    for h in range(2):
+        outward[h] = sender(
+            z_sum.at[1, :, halves[h]], z_in.at[0, :, halves[h]], z_s.at[h, 0], z_r.at[h, 0], near
+        )
+
+    @pl.when(middle)
+    def _():
+        def add_up(target, i, h, received):
+            span = slice(h * half, (h + 1) * half)
+            target[i, :, span] = (
+                z_out[i, :, span].astype(jnp.float32) + received[:, span].astype(jnp.float32)
+            ).astype(jnp.bfloat16)
+
+        for i, h in ((3, 0), (3, 1), (2, 0)):
+            inward[i, h].wait_recv()
+            add_up(z_sum, i, h, z_in.at[i])
+            crossing[i, h].start()
+        for h in range(2):
+            if h == 1:
+                inward[2, 1].wait_recv()
+                add_up(z_sum, 2, 1, z_in.at[2])
+                crossing[2, 1].start()
+            crossing[3, h].wait_recv()
+            add_up(z_sum, 1, h, z_across.at[3])
+            outward[h].start()
+        for h in range(2):
+            inward[1, h].wait_recv()
+            add_up(z_sum, 0, h, z_in.at[1])
+        for h in range(2):
+            crossing[2, h].wait_recv()
+        z_in[0] = (z_sum[0].astype(jnp.float32) + z_across[2].astype(jnp.float32)).astype(jnp.bfloat16)
+        z_sum[0] = z_in[0]
+
+    @pl.when(outer)
+    def _():
+        for h in range(2):
+            outward[h].wait_recv()
+        z_sum[0] = (z_out[0].astype(jnp.float32) + z_in[0].astype(jnp.float32)).astype(jnp.bfloat16)
+
+    summed = z_sum[0].astype(jnp.float32)
+    square_sum = square_out[0]
+    for k in range(1, n_z):
+        from_z = (me_z + k) % n_z
+        sender(
+            square_out.at[0], square_in.at[from_z], sq_s.at[0], sq_r.at[from_z], near
+        ).wait_recv()
+        square_sum = square_sum + square_in[pl.ds(from_z, 1)][0]
+    square_sum = jnp.concatenate(
+        [square_sum[:, j : j + 1] for j in range(piece // 8)], axis=0
+    )
+    inverse = lax.rsqrt(square_sum / (channels * n_tp) + EPSILON)
     residual_copy.wait()
     own = (res_rows[...].astype(jnp.float32) + summed * inverse).astype(jnp.bfloat16)
     own_ref[...] = own
@@ -520,8 +647,7 @@
     inverse = lax.rsqrt(jnp.mean(floated * floated, axis=1, keepdims=True) + EPSILON)
     normed_ref[...] = (floated * inverse * ffn_ref[...]).astype(jnp.bfloat16)
 
-    half = width // 2
-    lower, upper = pl.ds(0, half), pl.ds(half, half)
+    lower, upper = halves
     sent = []
 
     def push(source, target, sems, slot, peer):
@@ -532,27 +658,58 @@
 
     gz, gxy, gd, gp = (gz_s, gz_r), (gxy_s, gxy_r), (gd_s, gd_r), (gp_s, gp_r)
     rp, r1, r2, rz = (rp_s, rp_r), (r1_s, r1_r), (r2_s, r2_r), (rz_s, rz_r)
-    from_z, from_x, from_y, from_da, from_db, from_pair = {}, {}, {}, {}, {}, {}
+    from_x, from_y, from_da, from_db, from_pair = {}, {}, {}, {}, {}
+    mid_sent = []
+
+    def arrival(i):
+        block = blocks.at[i, me_s, me_c]
+        return sender(block, block, gz[0].at[i], gz[1].at[i], near)
+
+    def mid_push(source, i, slot, peer):
+        copy = sender(source, blocks.at[i, me_s, me_c], gz[0].at[slot], gz[1].at[i], peer)
+        pl.when(middle)(copy.start)
+        mid_sent.append(copy)
+
+    def pass_on(i):
+        pl.when(middle)(arrival(i).wait_recv)
+        mid_push(blocks.at[i, me_s, me_c], i, i + 2, near)
 
     def spread(i):
         block = blocks.at[i, me_s, me_c]
         if i == 0:
             source = normed_ref
+        elif i == 1:
+            arrival(1).wait_recv()
+            source = block
         else:
-            from_z[i].wait_recv()
+            pl.when(outer)(arrival(i).wait_recv)
             source = block
-        from_x[i] = push(source, block, gxy, (0, i), x_peer)
-        from_y[i] = push(source, block, gxy, (1, i), y_peer)
+        for h in range(2):
+            part, other = halves[h], halves[1 - h]
+            from_x[h, i] = push(source.at[:, part], block.at[:, part], gxy, (h, i), x_peer)
+            from_y[1 - h, i] = push(source.at[:, other], block.at[:, other], gxy, (3 - h, i), y_peer)
+        if i == 0:
+            sent.append(sender(source, blocks.at[1, me_s, me_c], gz[0].at[1], gz[1].at[1], near))
+            sent[-1].start()
+            mid_push(source, 2, 2, over)
+        elif i == 1:
+            mid_push(source, 3, 3, over)
         from_pair[0, i] = push(source, block, gp, (0, i), partner)
 
     def relay(i):
-        from_x[i].wait_recv()
-        block, part = blocks.at[i, s_x, me_c], blocks.at[i, s_x, me_c, :, lower]
+        from_x[0, i].wait_recv()
+        part = blocks.at[i, s_x, me_c, :, lower]
         from_da[i] = push(part, part, gd, (0, i), y_peer)
+        from_y[1, i].wait_recv()
+        part = blocks.at[i, s_y, me_c, :, upper]
+        from_db[i] = push(part, part, gd, (1, i), x_peer)
+
+    def share_xy(i):
+        from_x[1, i].wait_recv()
+        block = blocks.at[i, s_x, me_c]
         from_pair[1, i] = push(block, block, gp, (1, i), partner)
-        from_y[i].wait_recv()
-        block, part = blocks.at[i, s_y, me_c], blocks.at[i, s_y, me_c, :, upper]
-        from_db[i] = push(part, part, gd, (1, i), x_peer)
+        from_y[0, i].wait_recv()
+        block = blocks.at[i, s_y, me_c]
         from_pair[2, i] = push(block, block, gp, (2, i), partner)
 
     def hand_over(i):
@@ -566,8 +723,6 @@
     own_copy = pltpu.make_async_copy(normed_ref, blocks.at[0, me_s, me_c], own_sem)
     own_copy.start()
     spread(0)
-    for k in range(n_z - 1):
-        from_z[k + 1] = push(normed_ref, blocks.at[k + 1, me_s, me_c], gz, k, z_peers[k])
     for copy in share:
         copy.wait()
     for place in range(n_sp):
@@ -579,65 +734,62 @@
     ff = w_gate.shape[1]
     f_tile, d_tile = 256, min(512, width)
     count = n_sp * 2 * piece
-    back, first_xs, first_ys, second_xs, second_ys, back_z = {}, {}, {}, {}, {}, {}
-
-    def rise(i):
-        for k in range(5):
-            from_pair[k, i].wait_recv()
+    back, first_xs, first_ys, second_xs, second_ys = {}, {}, {}, {}, {}
+
+    def rise(i, step):
+        if step == 0:
+            for k in range(5):
+                from_pair[k, i].wait_recv()
         tokens = blocks[i].reshape(count, width)
-
-        def up_step(step, _):
-            span = pl.ds(pl.multiple_of(step * f_tile, f_tile), f_tile)
-            gate_part = jnp.dot(tokens, w_gate[:, span], preferred_element_type=jnp.float32)
-            up_part = jnp.dot(tokens, w_up[:, span], preferred_element_type=jnp.float32)
-            hidden_units[:, span] = (gate_part * jax.nn.sigmoid(gate_part) * up_part).astype(
-                jnp.bfloat16
-            )
-            return 0
-
-        lax.fori_loop(0, ff // f_tile, up_step, 0)
-
-    def fall(i):
+        span = slice(step * f_tile, (step + 1) * f_tile)
+        gate_part = jnp.dot(tokens, w_gate[:, span], preferred_element_type=jnp.float32)
+        up_part = jnp.dot(tokens, w_up[:, span], preferred_element_type=jnp.float32)
+        hidden_units[:, span] = (gate_part * jax.nn.sigmoid(gate_part) * up_part).astype(
+            jnp.bfloat16
+        )
+
+    targets = (s_d, s_x, s_y, me_s)
+
+    def fall(i, h):
         z = across[i]
         first = pl.multiple_of(z * (2 * piece), 2 * piece)
         scale = share_cols[:, pl.ds(first, 2 * piece), :].reshape(count, LANES)[:, :1]
         units = hidden_units[...]
-
-        def down_step(step, _):
-            span = pl.ds(pl.multiple_of(step * d_tile, d_tile), d_tile)
+        for step in range(half // d_tile):
+            begin = h * half + step * d_tile
+            span = slice(begin, begin + d_tile)
             product = jnp.dot(units, w_down[:, span], preferred_element_type=jnp.float32) * scale
             products[i, :, :, :, span] = product.astype(jnp.bfloat16).reshape(
                 n_sp, 2, piece, d_tile
             )
-            return 0
-
-        lax.fori_loop(0, width // d_tile, down_step, 0)
-        for k, group in enumerate((s_d, s_x, s_y, me_s)):
-            back[k, i] = push(
-                products.at[i, group, 1 - me_c], back_in.at[i, k], rp, (k, i), partner
+        for k, group in enumerate(targets):
+            back[k, h, i] = push(
+                products.at[i, group, 1 - me_c, :, halves[h]],
+                back_in.at[i, k, :, halves[h]],
+                rp,
+                (h * 4 + k, i),
+                partner,
             )
 
+    def merge(i, k, h):
+        span = slice(h * half, (h + 1) * half)
+        back[k, h, i].wait_recv()
+        joined[i, k, :, span] = (
+            products[i, targets[k], me_c, :, span].astype(jnp.float32)
+            + back_in[i, k, :, span].astype(jnp.float32)
+        ).astype(jnp.bfloat16)
+
     def join(i):
-        for k, group in enumerate((s_d, s_x, s_y, me_s)):
-            back[k, i].wait_recv()
-            joined[i, k] = (
-                products[i, group, me_c].astype(jnp.float32) + back_in[i, k].astype(jnp.float32)
-            ).astype(jnp.bfloat16)
-            if k == 0:
-                first_xs[1, i] = push(
-                    joined.at[i, 0, :, lower], first_x.at[1, i], r1, (2, i), x_peer
-                )
-                first_ys[1, i] = push(
-                    joined.at[i, 0, :, upper], first_y.at[1, i], r1, (3, i), y_peer
-                )
-            elif k == 1:
-                first_xs[0, i] = push(
-                    joined.at[i, 1, :, lower], first_x.at[0, i], r1, (0, i), x_peer
-                )
-            elif k == 2:
-                first_ys[0, i] = push(
-                    joined.at[i, 2, :, upper], first_y.at[0, i], r1, (1, i), y_peer
-                )
+        merge(i, 0, 0)
+        first_xs[1, i] = push(joined.at[i, 0, :, lower], first_x.at[1, i], r1, (2, i), x_peer)
+        merge(i, 0, 1)
+        first_ys[1, i] = push(joined.at[i, 0, :, upper], first_y.at[1, i], r1, (3, i), y_peer)
+        merge(i, 1, 0)
+        first_xs[0, i] = push(joined.at[i, 1, :, lower], first_x.at[0, i], r1, (0, i), x_peer)
+        merge(i, 2, 1)
+        first_ys[0, i] = push(joined.at[i, 2, :, upper], first_y.at[0, i], r1, (1, i), y_peer)
+        for k, h in ((2, 0), (1, 1), (3, 0), (3, 1)):
+            merge(i, k, h)
 
     def turn(i):
         first_xs[1, i].wait_recv()
@@ -669,35 +821,88 @@
         column[i] = jnp.concatenate([low, high], axis=1).astype(jnp.bfloat16)
         if i > 0:
             peer = z_peers[i - 1]
-            back_z[i] = push(column.at[i], last_in.at[i], rz, i, peer)
+            copy = sender(column.at[i], last_in.at[me_z], rz[0].at[i], rz[1].at[me_z], peer)
+            copy.start()
+            sent.append(copy)
 
     own_copy.wait()
     for copy in w_loads:
         copy.wait()
-    last = n_z - 1
-    spread(1)
-    for tick in range(-2, n_z + 2):
-        plan = (
-            (relay, tick + 2),
-            (spread, tick + 3),
-            (hand_over, tick + 1),
-            (rise, tick),
-            (join, tick - 1),
-            (finish, tick - 2),
-            (fall, tick),
-            (turn, tick - 1),
-        )
-        for stage, i in plan:
-            if 0 <= i <= last and not (stage is spread and i <= 1):
-                stage(i)
+    plan = (
+        (relay, 0),
+        (pass_on, 2),
+        (share_xy, 0),
+        (spread, 1),
+        (hand_over, 0),
+        (relay, 1),
+        (rise, 0, 0),
+        (rise, 0, 1),
+        (pass_on, 3),
+        (share_xy, 1),
+        (spread, 2),
+        (rise, 0, 2),
+        (fall, 0, 0),
+        (hand_over, 1),
+        (fall, 0, 1),
+        (relay, 2),
+        (rise, 1, 0),
+        (rise, 1, 1),
+        (share_xy, 2),
+        (spread, 3),
+        (rise, 1, 2),
+        (fall, 1, 0),
+        (hand_over, 2),
+        (fall, 1, 1),
+        (relay, 3),
+        (rise, 2, 0),
+        (rise, 2, 1),
+        (share_xy, 3),
+        (join, 1),
+        (rise, 2, 2),
+        (fall, 2, 0),
+        (hand_over, 3),
+        (fall, 2, 1),
+        (turn, 1),
+        (rise, 3, 0),
+        (rise, 3, 1),
+        (join, 2),
+        (finish, 1),
+        (rise, 3, 2),
+        (turn, 2),
+        (fall, 3, 0),
+        (fall, 3, 1),
+        (finish, 2),
+        (join, 3),
+        (join, 0),
+        (turn, 3),
+        (finish, 3),
+        (turn, 0),
+        (finish, 0),
+    )
+    for stage, *at in plan:
+        stage(*at)
     total = own_ref[...].astype(jnp.float32) + column[0].astype(jnp.float32)
-    for i in range(1, n_z):
-        back_z[i].wait_recv()
-        total = total + last_in[i].astype(jnp.float32)
+    for k in range(1, n_z):
+        z = (me_z + k) % n_z
+        sender(column.at[0], last_in.at[z], rz[0].at[0], rz[1].at[z], near).wait_recv()
+        total = total + last_in[pl.ds(z, 1)][0].astype(jnp.float32)
     out_ref[...] = total.astype(jnp.bfloat16)
-    for copies in pair + z_copies:
+    for copies in pair:
         for copy in copies:
             copy.wait_send()
+    for copy in square_copies:
+        copy.wait_send()
+
+    @pl.when(outer)
+    def _():
+        for copy in inward.values():
+            copy.wait_send()
+
+    @pl.when(middle)
+    def _():
+        for copy in list(crossing.values()) + list(outward.values()) + mid_sent:
+            copy.wait_send()
+
     for copy in sent:
         copy.wait_send()
 
@@ -737,15 +942,18 @@
     half_buffer = pltpu.VMEM((n_z, piece, half), bf16)
     chunks = pltpu.VMEM((n_z, n_sp, 2, piece, width), bf16)
     groups = pltpu.VMEM((n_z, n_sp, piece, width), bf16)
-    square_buffer = pltpu.VMEM((n_z, piece, LANES), f32)
+    square_buffer = pltpu.VMEM((n_z, 8, LANES), f32)
     shapes = (
-        [(2,)] * 2
-        + [(n_sp,)] * 4
-        + [(2, n_z)] * 4
+        [(n_sp,)] * 8
+        + [(2, n_z)] * 2
+        + [(2, n_z + 2)] * 2
         + [(n_z,)] * 2
-        + [(2, n_z)] * 4
+        + [(n_z + 2,)] * 2
+        + [(4, n_z)] * 2
+        + [(2, n_z)] * 2
         + [(5, n_z)] * 2
-        + [(4, n_z)] * 4
+        + [(8, n_z)] * 2
+        + [(4, n_z)] * 2
         + [(2, n_z)] * 2
         + [(n_z,)] * 2
     )
@@ -769,9 +977,13 @@
             pltpu.VMEM((top, rows), f32),
             pltpu.VMEM((rows, LANES), jnp.int32),
             pltpu.VMEM((padded, rows), f32),
-            pltpu.VMEM((16, channels), bf16),
+            pltpu.VMEM((32, channels), bf16),
+            pltpu.VMEM((n_sp, 32, channels), bf16),
             pltpu.VMEM((8, LANES), jnp.int32),
+            pltpu.VMEM((n_sp, 8, LANES), jnp.int32),
             pltpu.VMEM((8, channels), f32),
+            pltpu.VMEM((n_sp, 8, channels), f32),
+            pltpu.VMEM((n_sp, 8, channels), f32),
             pltpu.VMEM((n_sp, 8, channels), f32),
             pltpu.VMEM((n_sp, padded, rows), f32),
             pltpu.VMEM((rows, channels), f32),
@@ -780,7 +992,9 @@
             rows_buffer,
             rows_buffer,
             rows_buffer,
-            pltpu.VMEM((n_tp, piece, LANES), f32),
+            rows_buffer,
+            rows_buffer,
+            pltpu.VMEM((n_tp, 8, LANES), f32),
             square_buffer,
             square_buffer,
             square_buffer,

time: 87.1 us -> 76.8 us (0.88)
  Pallas kernels: 85.4 us -> 75 us
    pallas_call x1, Pallas kernels: 85.4 us -> 75 us  [dense_local(): pl.pallas_call(functools.partial(layer_kernel, n_sp, n_tp), out_shape=jax...]
where the time goes in v1:
time: 76.8 us; the launch traced here: 76.6 us
  Pallas kernels  75 us (98%)
  local copies, waits for them, and re-layouts  1.57 us (2%)
    pallas_call x1, Pallas kernels, dense_local(): pl.pallas_call(functools.partial(layer_kernel, n_sp, n_tp), out_shape=jax...  75 us
    unnamed x1, local copies, waits for them, and re-layouts  1.57 us

profile of v1, /device:TPU:0, one launch (start us, length us, event | category | flops | bytes accessed | tf_op | source)
XLA Modules:
  0.0 76.6 jit_solution(17881354449029104423)
XLA Ops:
  0.0 75.0 %shard_map.154 = bf16[32,2048]{1,0:T(8,128)(2,1)} custom-call(bf16[256,256]{1,0:T(8,128)(2,1)} %lru_hbm.1, bf16[256,256]{1,0:T(8,128)(2,1)} %gate_hbm.1, s32[1,256]{1,0:T(1,128)} %bitcast.15, bf16[4,256]{1,0:T(4,128)(2,1)} %taps_hbm.1, bf16[2,128,128]{2,1,0:T(8,128)(2,1)} %rate_hbm.1, bf16[2,128,128]{2,1,0:T(8,128)(2,1)} %inlet_hbm.1, f32[1,256]{1,0:T(1,128)} %bitcast.16, ...), custom_call_target="tpu_custom_call" | custom-call | tf_op jit(solution)/shard_map/pallas_call | solution.py:960
  75.0 1.6 %copy.18 = bf16[32,2048]{1,0:T(8,128)(2,1)} copy(bf16[32,2048]{1,0:T(8,128)(2,1)} %shard_map.154) | data formatting | bytes 262144

commit v2 on v1

--- a/solution.py
+++ b/solution.py
@@ -294,8 +294,6 @@
     share_cols,
     blocks,
     hidden_units,
-    products,
-    back_in,
     joined,
     first_x,
     first_y,
@@ -303,6 +301,7 @@
     second_y,
     relay_a,
     relay_b,
+    relay_c,
     column,
     last_in,
     load_sem,
@@ -329,10 +328,8 @@
     gxy_r,
     gd_s,
     gd_r,
-    gp_s,
-    gp_r,
-    rp_s,
-    rp_r,
+    wp_s,
+    wp_r,
     r1_s,
     r1_r,
     r2_s,
@@ -373,7 +370,11 @@
     w_loads = [
         pltpu.make_async_copy(source, target, w_sem.at[k])
         for k, (source, target) in enumerate(
-            ((w_gate_hbm, w_gate), (w_up_hbm, w_up), (w_down_hbm, w_down))
+            (
+                (w_gate_hbm, w_gate.at[me_c]),
+                (w_up_hbm, w_up.at[me_c]),
+                (w_down_hbm, w_down.at[me_c]),
+            )
         )
     ]
     s_x = me_s + 1 - 2 * (me_s % 2)
@@ -453,6 +454,10 @@
         ]
     for copy in carry:
         copy.start()
+    w_swaps = [
+        sender(part.at[me_c], part.at[me_c], wp_s.at[k], wp_r.at[k], partner)
+        for k, part in enumerate((w_gate, w_up, w_down))
+    ]
     carry_in[pl.ds(me_s, 1)] = carry_out[...][None]
     mark_in[pl.ds(me_s, 1)] = mark_out[...][None]
     edge_in[pl.ds(me_s, 1)] = edge_out[...][None]
@@ -477,6 +482,8 @@
     raw = gate_ref[...].astype(jnp.float32)
     gelu = 0.5 * raw * (1.0 + jnp.tanh(GELU_SCALE * (raw + 0.044715 * raw * raw * raw)))
     gelu = gelu * gain_ref[...]
+    w_loads[0].wait()
+    w_swaps[0].start()
     for copy in carry:
         copy.wait()
     xs, now, prior = [], [], []
@@ -583,6 +590,9 @@
                 for h in range(2):
                     inward[i, h].start()
 
+    for k in (1, 2):
+        w_loads[k].wait()
+        w_swaps[k].start()
     crossing, outward = {}, {}
     for i in (3, 2):
         for h in range(2):
@@ -656,71 +666,80 @@
         sent.append(copy)
         return copy
 
-    gz, gxy, gd, gp = (gz_s, gz_r), (gxy_s, gxy_r), (gd_s, gd_r), (gp_s, gp_r)
-    rp, r1, r2, rz = (rp_s, rp_r), (r1_s, r1_r), (r2_s, r2_r), (rz_s, rz_r)
-    from_x, from_y, from_da, from_db, from_pair = {}, {}, {}, {}, {}
+    gz, gxy, gd = (gz_s, gz_r), (gxy_s, gxy_r), (gd_s, gd_r)
+    r1, r2, rz = (r1_s, r1_r), (r2_s, r2_r), (rz_s, rz_r)
+    from_x, from_y, from_da, from_db = {}, {}, {}, {}
     mid_sent = []
 
-    def arrival(i):
-        block = blocks.at[i, me_s, me_c]
-        return sender(block, block, gz[0].at[i], gz[1].at[i], near)
-
-    def mid_push(source, i, slot, peer):
-        copy = sender(source, blocks.at[i, me_s, me_c], gz[0].at[slot], gz[1].at[i], peer)
+    def arrival(i, h):
+        part = blocks.at[i, me_s, :, halves[h]]
+        return sender(part, part, gz[0].at[h, i], gz[1].at[h, i], near)
+
+    def mid_push(source, i, h, slot, peer):
+        part = blocks.at[i, me_s, :, halves[h]]
+        copy = sender(source.at[:, halves[h]], part, gz[0].at[h, slot], gz[1].at[h, i], peer)
         pl.when(middle)(copy.start)
         mid_sent.append(copy)
 
-    def pass_on(i):
-        pl.when(middle)(arrival(i).wait_recv)
-        mid_push(blocks.at[i, me_s, me_c], i, i + 2, near)
+    def pass_on(i, h):
+        pl.when(middle)(arrival(i, h).wait_recv)
+        mid_push(blocks.at[i, me_s], i, h, i + 2, near)
 
     def spread(i):
-        block = blocks.at[i, me_s, me_c]
+        block = blocks.at[i, me_s]
+        source = normed_ref if i == 0 else block
+
+        def ready(h):
+            if i == 1:
+                arrival(1, h).wait_recv()
+                mid_push(source, 3, h, 3, over)
+            elif i > 1:
+                pl.when(outer)(arrival(i, h).wait_recv)
+
+        def to_x(h):
+            part = halves[h]
+            from_x[h, i] = push(source.at[:, part], block.at[:, part], gxy, (h, i), x_peer)
+
+        def to_y(h):
+            part = halves[h]
+            from_y[h, i] = push(source.at[:, part], block.at[:, part], gxy, (2 + h, i), y_peer)
+
+        ready(0)
+        to_x(0)
+        ready(1)
+        to_y(1)
+        to_x(1)
+        to_y(0)
         if i == 0:
-            source = normed_ref
-        elif i == 1:
-            arrival(1).wait_recv()
-            source = block
-        else:
-            pl.when(outer)(arrival(i).wait_recv)
-            source = block
-        for h in range(2):
-            part, other = halves[h], halves[1 - h]
-            from_x[h, i] = push(source.at[:, part], block.at[:, part], gxy, (h, i), x_peer)
-            from_y[1 - h, i] = push(source.at[:, other], block.at[:, other], gxy, (3 - h, i), y_peer)
-        if i == 0:
-            sent.append(sender(source, blocks.at[1, me_s, me_c], gz[0].at[1], gz[1].at[1], near))
-            sent[-1].start()
-            mid_push(source, 2, 2, over)
-        elif i == 1:
-            mid_push(source, 3, 3, over)
-        from_pair[0, i] = push(source, block, gp, (0, i), partner)
+            for h in range(2):
+                part = halves[h]
+                sent.append(
+                    sender(
+                        source.at[:, part],
+                        blocks.at[1, me_s, :, part],
+                        gz[0].at[h, 1],
+                        gz[1].at[h, 1],
+                        near,
+                    )
+                )
+                sent[-1].start()
+                mid_push(source, 2, h, 2, over)
 
     def relay(i):
         from_x[0, i].wait_recv()
-        part = blocks.at[i, s_x, me_c, :, lower]
+        part = blocks.at[i, s_x, :, lower]
         from_da[i] = push(part, part, gd, (0, i), y_peer)
         from_y[1, i].wait_recv()
-        part = blocks.at[i, s_y, me_c, :, upper]
+        part = blocks.at[i, s_y, :, upper]
         from_db[i] = push(part, part, gd, (1, i), x_peer)
 
-    def share_xy(i):
+    def gathered(i):
         from_x[1, i].wait_recv()
-        block = blocks.at[i, s_x, me_c]
-        from_pair[1, i] = push(block, block, gp, (1, i), partner)
         from_y[0, i].wait_recv()
-        block = blocks.at[i, s_y, me_c]
-        from_pair[2, i] = push(block, block, gp, (2, i), partner)
-
-    def hand_over(i):
         from_da[i].wait_recv()
-        part = blocks.at[i, s_d, me_c, :, lower]
-        from_pair[3, i] = push(part, part, gp, (3, i), partner)
         from_db[i].wait_recv()
-        part = blocks.at[i, s_d, me_c, :, upper]
-        from_pair[4, i] = push(part, part, gp, (4, i), partner)
-
-    own_copy = pltpu.make_async_copy(normed_ref, blocks.at[0, me_s, me_c], own_sem)
+
+    own_copy = pltpu.make_async_copy(normed_ref, blocks.at[0, me_s], own_sem)
     own_copy.start()
     spread(0)
     for copy in share:
@@ -731,75 +750,58 @@
         chosen = jnp.sum(jnp.where(lane == me_s, turned, 0.0), axis=1, keepdims=True)
         share_cols[place] = jnp.broadcast_to(chosen, (rows, LANES))
 
-    ff = w_gate.shape[1]
+    ff = w_gate.shape[2]
     f_tile, d_tile = 256, min(512, width)
-    count = n_sp * 2 * piece
-    back, first_xs, first_ys, second_xs, second_ys = {}, {}, {}, {}, {}
+    count = n_sp * piece
+    first_xs, first_ys, second_xs, second_ys = {}, {}, {}, {}
+    slabs = ff // f_tile
+
+    def swapped(k):
+        w_swaps[k].wait_recv()
 
     def rise(i, step):
-        if step == 0:
-            for k in range(5):
-                from_pair[k, i].wait_recv()
         tokens = blocks[i].reshape(count, width)
-        span = slice(step * f_tile, (step + 1) * f_tile)
-        gate_part = jnp.dot(tokens, w_gate[:, span], preferred_element_type=jnp.float32)
-        up_part = jnp.dot(tokens, w_up[:, span], preferred_element_type=jnp.float32)
-        hidden_units[:, span] = (gate_part * jax.nn.sigmoid(gate_part) * up_part).astype(
-            jnp.bfloat16
-        )
-
-    targets = (s_d, s_x, s_y, me_s)
+        for tile in (2 * step, 2 * step + 1):
+            core, span = tile // slabs, pl.ds(tile % slabs * f_tile, f_tile)
+            gate_part = jnp.dot(tokens, w_gate[core, :, span], preferred_element_type=jnp.float32)
+            up_part = jnp.dot(tokens, w_up[core, :, span], preferred_element_type=jnp.float32)
+            hidden_units[:, tile * f_tile : (tile + 1) * f_tile] = (
+                gate_part * jax.nn.sigmoid(gate_part) * up_part
+            ).astype(jnp.bfloat16)
 
     def fall(i, h):
-        z = across[i]
-        first = pl.multiple_of(z * (2 * piece), 2 * piece)
-        scale = share_cols[:, pl.ds(first, 2 * piece), :].reshape(count, LANES)[:, :1]
+        first = pl.multiple_of(across[i] * (2 * piece) + me_c * piece, piece)
+        scale = share_cols[:, pl.ds(first, piece), :].reshape(count, LANES)[:, :1]
         units = hidden_units[...]
         for step in range(half // d_tile):
             begin = h * half + step * d_tile
             span = slice(begin, begin + d_tile)
-            product = jnp.dot(units, w_down[:, span], preferred_element_type=jnp.float32) * scale
-            products[i, :, :, :, span] = product.astype(jnp.bfloat16).reshape(
-                n_sp, 2, piece, d_tile
+            product = jnp.dot(
+                units,
+                w_down[:, :, span].reshape(2 * ff, d_tile),
+                preferred_element_type=jnp.float32,
             )
-        for k, group in enumerate(targets):
-            back[k, h, i] = push(
-                products.at[i, group, 1 - me_c, :, halves[h]],
-                back_in.at[i, k, :, halves[h]],
-                rp,
-                (h * 4 + k, i),
-                partner,
+            joined[i, :, :, span] = (
+                (product * scale).astype(jnp.bfloat16).reshape(n_sp, piece, d_tile)
             )
 
-    def merge(i, k, h):
-        span = slice(h * half, (h + 1) * half)
-        back[k, h, i].wait_recv()
-        joined[i, k, :, span] = (
-            products[i, targets[k], me_c, :, span].astype(jnp.float32)
-            + back_in[i, k, :, span].astype(jnp.float32)
-        ).astype(jnp.bfloat16)
-
-    def join(i):
-        merge(i, 0, 0)
-        first_xs[1, i] = push(joined.at[i, 0, :, lower], first_x.at[1, i], r1, (2, i), x_peer)
-        merge(i, 0, 1)
-        first_ys[1, i] = push(joined.at[i, 0, :, upper], first_y.at[1, i], r1, (3, i), y_peer)
-        merge(i, 1, 0)
-        first_xs[0, i] = push(joined.at[i, 1, :, lower], first_x.at[0, i], r1, (0, i), x_peer)
-        merge(i, 2, 1)
-        first_ys[0, i] = push(joined.at[i, 2, :, upper], first_y.at[0, i], r1, (1, i), y_peer)
-        for k, h in ((2, 0), (1, 1), (3, 0), (3, 1)):
-            merge(i, k, h)
+    def depart(i, h):
+        if h == 0:
+            first_xs[1, i] = push(joined.at[i, s_d, :, lower], first_x.at[1, i], r1, (2, i), x_peer)
+            first_xs[0, i] = push(joined.at[i, s_x, :, lower], first_x.at[0, i], r1, (0, i), x_peer)
+        else:
+            first_ys[1, i] = push(joined.at[i, s_d, :, upper], first_y.at[1, i], r1, (3, i), y_peer)
+            first_ys[0, i] = push(joined.at[i, s_y, :, upper], first_y.at[0, i], r1, (1, i), y_peer)
 
     def turn(i):
         first_xs[1, i].wait_recv()
         relay_a[i] = (
-            joined[i, 2, :, :half].astype(jnp.float32) + first_x[1, i].astype(jnp.float32)
+            joined[i, s_y, :, :half].astype(jnp.float32) + first_x[1, i].astype(jnp.float32)
         ).astype(jnp.bfloat16)
         second_ys[i] = push(relay_a.at[i], second_y.at[i], r2, (0, i), y_peer)
         first_ys[1, i].wait_recv()
         relay_b[i] = (
-            joined[i, 1, :, half:].astype(jnp.float32) + first_y[1, i].astype(jnp.float32)
+            joined[i, s_x, :, half:].astype(jnp.float32) + first_y[1, i].astype(jnp.float32)
         ).astype(jnp.bfloat16)
         second_xs[i] = push(relay_b.at[i], second_x.at[i], r2, (1, i), x_peer)
 
@@ -809,98 +811,161 @@
         for copies in (second_xs, second_ys):
             copies[i].wait_recv()
         low = (
-            joined[i, 3, :, :half].astype(jnp.float32)
+            joined[i, me_s, :, :half].astype(jnp.float32)
             + first_x[0, i].astype(jnp.float32)
             + second_y[i].astype(jnp.float32)
         )
         high = (
-            joined[i, 3, :, half:].astype(jnp.float32)
+            joined[i, me_s, :, half:].astype(jnp.float32)
             + first_y[0, i].astype(jnp.float32)
             + second_x[i].astype(jnp.float32)
         )
         column[i] = jnp.concatenate([low, high], axis=1).astype(jnp.bfloat16)
-        if i > 0:
-            peer = z_peers[i - 1]
-            copy = sender(column.at[i], last_in.at[me_z], rz[0].at[i], rz[1].at[me_z], peer)
+        if i in (1, 3):
+            copy = sender(
+                column.at[i], last_in.at[me_z], rz[0].at[0, i], rz[1].at[0, me_z], z_peers[i - 1]
+            )
             copy.start()
             sent.append(copy)
+        elif i == 2:
+            for h in range(2):
+                pl.when(outer)(homeward[h].start)
+
+    homeward, crossed = [], []
+    for h in range(2):
+        part = halves[h]
+        homeward.append(
+            sender(
+                column.at[2, :, part],
+                last_in.at[z_near, :, part],
+                rz[0].at[h, 2],
+                rz[1].at[h, z_near],
+                near,
+            )
+        )
+        crossed.append(
+            sender(
+                relay_c.at[:, part],
+                last_in.at[me_z, :, part],
+                rz[0].at[h, 2],
+                rz[1].at[h, me_z],
+                over,
+            )
+        )
+
+    def cross(i):
+        @pl.when(middle)
+        def _():
+            for h in range(2):
+                span = slice(h * half, (h + 1) * half)
+                part = last_in.at[me_z, :, halves[h]]
+                sender(part, part, rz[0].at[h, 2], rz[1].at[h, me_z], near).wait_recv()
+                relay_c[:, span] = (
+                    column[i, :, span].astype(jnp.float32)
+                    + last_in[me_z, :, span].astype(jnp.float32)
+                ).astype(jnp.bfloat16)
+                crossed[h].start()
 
     own_copy.wait()
-    for copy in w_loads:
-        copy.wait()
     plan = (
         (relay, 0),
-        (pass_on, 2),
-        (share_xy, 0),
+        (pass_on, 2, 0),
+        (pass_on, 2, 1),
         (spread, 1),
-        (hand_over, 0),
+        (gathered, 0),
+        (swapped, 0),
+        (swapped, 1),
+        (rise, 0, 0),
         (relay, 1),
-        (rise, 0, 0),
         (rise, 0, 1),
-        (pass_on, 3),
-        (share_xy, 1),
         (spread, 2),
+        (pass_on, 3, 0),
+        (pass_on, 3, 1),
         (rise, 0, 2),
+        (swapped, 2),
         (fall, 0, 0),
-        (hand_over, 1),
         (fall, 0, 1),
+        (gathered, 1),
+        (rise, 1, 0),
         (relay, 2),
-        (rise, 1, 0),
         (rise, 1, 1),
-        (share_xy, 2),
         (spread, 3),
         (rise, 1, 2),
         (fall, 1, 0),
-        (hand_over, 2),
         (fall, 1, 1),
-        (relay, 3),
+        (gathered, 2),
         (rise, 2, 0),
         (rise, 2, 1),
-        (share_xy, 3),
-        (join, 1),
+        (relay, 3),
+        (depart, 1, 0),
+        (depart, 1, 1),
         (rise, 2, 2),
         (fall, 2, 0),
-        (hand_over, 3),
+        (depart, 2, 0),
         (fall, 2, 1),
+        (depart, 2, 1),
+        (gathered, 3),
+        (rise, 3, 0),
         (turn, 1),
-        (rise, 3, 0),
         (rise, 3, 1),
-        (join, 2),
+        (rise, 3, 2),
+        (fall, 3, 0),
+        (depart, 3, 0),
+        (fall, 3, 1),
+        (depart, 3, 1),
+        (turn, 2),
         (finish, 1),
-        (rise, 3, 2),
-        (turn, 2),
-        (fall, 3, 0),
-        (fall, 3, 1),
+        (turn, 3),
+        (depart, 0, 0),
+        (depart, 0, 1),
         (finish, 2),
-        (join, 3),
-        (join, 0),
-        (turn, 3),
         (finish, 3),
         (turn, 0),
+        (cross, 2),
         (finish, 0),
     )
     for stage, *at in plan:
         stage(*at)
     total = own_ref[...].astype(jnp.float32) + column[0].astype(jnp.float32)
-    for k in range(1, n_z):
-        z = (me_z + k) % n_z
-        sender(column.at[0], last_in.at[z], rz[0].at[0], rz[1].at[z], near).wait_recv()
-        total = total + last_in[pl.ds(z, 1)][0].astype(jnp.float32)
+    def landed(h, z):
+        if h is None:
+            sender(column.at[0], last_in.at[z], rz[0].at[0, 0], rz[1].at[0, z], near).wait_recv()
+        else:
+            part = last_in.at[z, :, halves[h]]
+            sender(part, part, rz[0].at[h, 0], rz[1].at[h, z], near).wait_recv()
+
+    landed(None, z_near)
+    total = total + last_in[z_near].astype(jnp.float32)
+
+    @pl.when(outer)
+    def _():
+        landed(None, across[2])
+        landed(None, z_far)
+
+    @pl.when(middle)
+    def _():
+        landed(0, z_far)
+        landed(1, z_far)
+        last_in[me_z] = jnp.zeros(last_in.shape[1:], last_in.dtype)
+
+    total = total + last_in[z_far].astype(jnp.float32)
+    last = jnp.where(middle, me_z, across[2])
+    total = total + last_in[pl.ds(last, 1)][0].astype(jnp.float32)
     out_ref[...] = total.astype(jnp.bfloat16)
     for copies in pair:
         for copy in copies:
             copy.wait_send()
-    for copy in square_copies:
+    for copy in square_copies + w_swaps:
         copy.wait_send()
 
     @pl.when(outer)
     def _():
-        for copy in inward.values():
+        for copy in list(inward.values()) + homeward:
             copy.wait_send()
 
     @pl.when(middle)
     def _():
-        for copy in list(crossing.values()) + list(outward.values()) + mid_sent:
+        for copy in list(crossing.values()) + list(outward.values()) + mid_sent + crossed:
             copy.wait_send()
 
     for copy in sent:
@@ -940,7 +1005,6 @@
     dma = pltpu.SemaphoreType.DMA
     rows_buffer = pltpu.VMEM((n_z, piece, width), bf16)
     half_buffer = pltpu.VMEM((n_z, piece, half), bf16)
-    chunks = pltpu.VMEM((n_z, n_sp, 2, piece, width), bf16)
     groups = pltpu.VMEM((n_z, n_sp, piece, width), bf16)
     square_buffer = pltpu.VMEM((n_z, 8, LANES), f32)
     shapes = (
@@ -948,14 +1012,13 @@
         + [(2, n_z)] * 2
         + [(2, n_z + 2)] * 2
         + [(n_z,)] * 2
-        + [(n_z + 2,)] * 2
+        + [(2, n_z + 2)] * 2
         + [(4, n_z)] * 2
         + [(2, n_z)] * 2
-        + [(5, n_z)] * 2
-        + [(8, n_z)] * 2
+        + [(3,)] * 2
         + [(4, n_z)] * 2
         + [(2, n_z)] * 2
-        + [(n_z,)] * 2
+        + [(2, n_z)] * 2
     )
     return pl.pallas_call(
         functools.partial(layer_kernel, n_sp, n_tp),
@@ -1001,14 +1064,12 @@
             pltpu.VMEM((piece, width), bf16),
             pltpu.VMEM((piece, width), bf16),
             pltpu.VMEM((piece, width), bf16),
-            pltpu.VMEM((width, ff), bf16),
-            pltpu.VMEM((width, ff), bf16),
-            pltpu.VMEM((ff, width), bf16),
+            pltpu.VMEM((2, width, ff), bf16),
+            pltpu.VMEM((2, width, ff), bf16),
+            pltpu.VMEM((2, ff, width), bf16),
             pltpu.VMEM((n_sp, rows, LANES), f32),
-            chunks,
-            pltpu.VMEM((n_sp * 2 * piece, ff), bf16),
-            chunks,
             groups,
+            pltpu.VMEM((n_sp * piece, 2 * ff), bf16),
             groups,
             pltpu.VMEM((2, n_z, piece, half), bf16),
             pltpu.VMEM((2, n_z, piece, half), bf16),
@@ -1016,6 +1077,7 @@
             half_buffer,
             half_buffer,
             half_buffer,
+            pltpu.VMEM((piece, width), bf16),
             rows_buffer,
             rows_buffer,
             dma((12,)),

time: 76.8 us -> 68.3 us (0.89)
  Pallas kernels: 75 us -> 66.6 us
    pallas_call x1, Pallas kernels: 75 us -> 66.6 us  [dense_local(): pl.pallas_call(functools.partial(layer_kernel, n_sp, n_tp), out_shape=jax...]
where the time goes in v2:
time: 68.3 us; the launch traced here: 68.1 us
  Pallas kernels  66.6 us (98%)
  local copies, waits for them, and re-layouts  1.57 us (2%)
    pallas_call x1, Pallas kernels, dense_local(): pl.pallas_call(functools.partial(layer_kernel, n_sp, n_tp), out_shape=jax...  66.6 us
    unnamed x1, local copies, waits for them, and re-layouts  1.57 us

profile of v2, /device:TPU:0, one launch (start us, length us, event | category | flops | bytes accessed | tf_op | source)
XLA Modules:
  0.0 68.1 jit_solution(17855171952628698781)
XLA Ops:
  0.0 66.6 %shard_map.154 = bf16[32,2048]{1,0:T(8,128)(2,1)} custom-call(bf16[256,256]{1,0:T(8,128)(2,1)} %lru_hbm.1, bf16[256,256]{1,0:T(8,128)(2,1)} %gate_hbm.1, s32[1,256]{1,0:T(1,128)} %bitcast.15, bf16[4,256]{1,0:T(4,128)(2,1)} %taps_hbm.1, bf16[2,128,128]{2,1,0:T(8,128)(2,1)} %rate_hbm.1, bf16[2,128,128]{2,1,0:T(8,128)(2,1)} %inlet_hbm.1, f32[1,256]{1,0:T(1,128)} %bitcast.16, ...), custom_call_target="tpu_custom_call" | custom-call | tf_op jit(solution)/shard_map/pallas_call | solution.py:1023
  66.6 1.6 %copy.18 = bf16[32,2048]{1,0:T(8,128)(2,1)} copy(bf16[32,2048]{1,0:T(8,128)(2,1)} %shard_map.154) | data formatting | bytes 262144

commit v3 on v2

--- a/solution.py
+++ b/solution.py
@@ -403,8 +403,8 @@
     docs_ref[...] = docs
     lane8 = lax.broadcasted_iota(jnp.int32, (8, LANES), 1)
     mark_out[...] = jnp.where(lane8 == 0, docs[:8], docs[rows - 8 :])
-    edge_out[0:16] = lru_ref[0:16]
-    edge_out[16:32] = lru_ref[rows - 16 :]
+    edge_out[0:8] = lru_ref[0:8]
+    edge_out[8:16] = lru_ref[rows - 8 :]
     taps = taps_ref[...].astype(jnp.float32)
     reach = taps.shape[0] - 1
 
@@ -482,8 +482,6 @@
     raw = gate_ref[...].astype(jnp.float32)
     gelu = 0.5 * raw * (1.0 + jnp.tanh(GELU_SCALE * (raw + 0.044715 * raw * raw * raw)))
     gelu = gelu * gain_ref[...]
-    w_loads[0].wait()
-    w_swaps[0].start()
     for copy in carry:
         copy.wait()
     xs, now, prior = [], [], []
@@ -497,7 +495,7 @@
         xs.append(
             jnp.concatenate(
                 [
-                    edge_in[max(place - 1, 0)].astype(jnp.float32)[24:],
+                    edge_in[max(place - 1, 0)].astype(jnp.float32)[8:],
                     edge_in[place].astype(jnp.float32)[:8],
                 ],
                 axis=0,
@@ -590,7 +588,7 @@
                 for h in range(2):
                     inward[i, h].start()
 
-    for k in (1, 2):
+    for k in range(3):
         w_loads[k].wait()
         w_swaps[k].start()
     crossing, outward = {}, {}
@@ -1000,7 +998,7 @@
     vmem = pl.BlockSpec(memory_space=pltpu.VMEM)
     half = width // 2
     top = routes.shape[1]
-    hbm = pl.BlockSpec(memory_space=pl.ANY)
+    hbm = pl.BlockSpec(memory_space=pltpu.HBM)
     bf16, f32 = jnp.bfloat16, jnp.float32
     dma = pltpu.SemaphoreType.DMA
     rows_buffer = pltpu.VMEM((n_z, piece, width), bf16)
@@ -1022,7 +1020,7 @@
     )
     return pl.pallas_call(
         functools.partial(layer_kernel, n_sp, n_tp),
-        out_shape=jax.ShapeDtypeStruct((piece, width), bf16),
+        out_shape=pltpu.VMEM((piece, width), bf16),
         in_specs=[hbm] * 16,
         out_specs=vmem,
         scratch_shapes=[
@@ -1040,8 +1038,8 @@
             pltpu.VMEM((top, rows), f32),
             pltpu.VMEM((rows, LANES), jnp.int32),
             pltpu.VMEM((padded, rows), f32),
-            pltpu.VMEM((32, channels), bf16),
-            pltpu.VMEM((n_sp, 32, channels), bf16),
+            pltpu.VMEM((16, channels), bf16),
+            pltpu.VMEM((n_sp, 16, channels), bf16),
             pltpu.VMEM((8, LANES), jnp.int32),
             pltpu.VMEM((n_sp, 8, LANES), jnp.int32),
             pltpu.VMEM((8, channels), f32),
@@ -1087,9 +1085,10 @@
         ]
         + [dma(shape) for shape in shapes],
         compiler_params=pltpu.CompilerParams(
-            collective_id=0, has_side_effects=True, vmem_limit_bytes=60 * 2**20
+            collective_id=0, has_side_effects=True, vmem_limit_bytes=48 * 2**20
         ),
     )(
+        *(pltpu.with_memory_space_constraint(operand, pltpu.HBM) for operand in (
         lru_input,
         gate_input,
         documents[None, :],
@@ -1106,6 +1105,7 @@
         w_gate[0],
         w_up[0],
         w_down[0],
+        ))
     )
 
 

time: 68.3 us -> 66.2 us (0.969)
  Pallas kernels: 66.6 us -> 65.4 us
  local copies, waits for them, and re-layouts: 1.57 us -> 0.66 us
    pallas_call x1, Pallas kernels: 66.6 us -> 65.4 us  [dense_local(): pl.pallas_call(functools.partial(layer_kernel, n_sp, n_tp), out_shape=plt...]
    unnamed x1, local copies, waits for them, and re-layouts: 1.57 us -> 0.66 us
where the time goes in v3:
time: 66.2 us; the launch traced here: 66.1 us
  Pallas kernels  65.4 us (99%)
    pallas_call x1, Pallas kernels, dense_local(): pl.pallas_call(functools.partial(layer_kernel, n_sp, n_tp), out_shape=plt...  65.4 us

profile of v3, /device:TPU:0, one launch (start us, length us, event | category | flops | bytes accessed | tf_op | source)
XLA Modules:
  0.0 66.1 jit_solution(13064508035007444968)
XLA Ops:
  0.0 65.4 %shard_map.154 = bf16[32,2048]{1,0:T(8,128)(2,1)S(1)} custom-call(bf16[256,256]{1,0:T(8,128)(2,1)} %lru_hbm.1, bf16[256,256]{1,0:T(8,128)(2,1)} %gate_hbm.1, s32[1,256]{1,0:T(1,128)} %bitcast.15, bf16[4,256]{1,0:T(4,128)(2,1)} %taps_hbm.1, bf16[2,128,128]{2,1,0:T(8,128)(2,1)} %rate_hbm.1, bf16[2,128,128]{2,1,0:T(8,128)(2,1)} %inlet_hbm.1, ...), custom_call_target="tpu_custom_call" | custom-call | tf_op jit(solution)/shard_map/pallas_call | solution.py:1021
  65.4 0.7 copy.18

commit v4 on v3

--- a/solution.py
+++ b/solution.py
@@ -403,8 +403,8 @@
     docs_ref[...] = docs
     lane8 = lax.broadcasted_iota(jnp.int32, (8, LANES), 1)
     mark_out[...] = jnp.where(lane8 == 0, docs[:8], docs[rows - 8 :])
-    edge_out[0:8] = lru_ref[0:8]
-    edge_out[8:16] = lru_ref[rows - 8 :]
+    edge_out[0:16] = lru_ref[0:16]
+    edge_out[16:32] = lru_ref[rows - 16 :]
     taps = taps_ref[...].astype(jnp.float32)
     reach = taps.shape[0] - 1
 
@@ -495,7 +495,7 @@
         xs.append(
             jnp.concatenate(
                 [
-                    edge_in[max(place - 1, 0)].astype(jnp.float32)[8:],
+                    edge_in[max(place - 1, 0)].astype(jnp.float32)[24:],
                     edge_in[place].astype(jnp.float32)[:8],
                 ],
                 axis=0,
@@ -1038,8 +1038,8 @@
             pltpu.VMEM((top, rows), f32),
             pltpu.VMEM((rows, LANES), jnp.int32),
             pltpu.VMEM((padded, rows), f32),
-            pltpu.VMEM((16, channels), bf16),
-            pltpu.VMEM((n_sp, 16, channels), bf16),
+            pltpu.VMEM((32, channels), bf16),
+            pltpu.VMEM((n_sp, 32, channels), bf16),
             pltpu.VMEM((8, LANES), jnp.int32),
             pltpu.VMEM((n_sp, 8, LANES), jnp.int32),
             pltpu.VMEM((8, channels), f32),

time: 66.2 us -> 66.5 us (level)
  no operation moved by 1% of the time
where the time goes in v4:
time: 66.5 us; the launch traced here: 66.4 us
  Pallas kernels  65.7 us (99%)
    pallas_call x1, Pallas kernels, dense_local(): pl.pallas_call(functools.partial(layer_kernel, n_sp, n_tp), out_shape=plt...  65.7 us

profile of v4, /device:TPU:0, one launch (start us, length us, event | category | flops | bytes accessed | tf_op | source)
XLA Modules:
  0.0 66.4 jit_solution(1899646247501178116)
XLA Ops:
  0.0 65.7 %shard_map.154 = bf16[32,2048]{1,0:T(8,128)(2,1)S(1)} custom-call(bf16[256,256]{1,0:T(8,128)(2,1)} %lru_hbm.1, bf16[256,256]{1,0:T(8,128)(2,1)} %gate_hbm.1, s32[1,256]{1,0:T(1,128)} %bitcast.15, bf16[4,256]{1,0:T(4,128)(2,1)} %taps_hbm.1, bf16[2,128,128]{2,1,0:T(8,128)(2,1)} %rate_hbm.1, bf16[2,128,128]{2,1,0:T(8,128)(2,1)} %inlet_hbm.1, ...), custom_call_target="tpu_custom_call" | custom-call | tf_op jit(solution)/shard_map/pallas_call | solution.py:1021
  65.7 0.7 copy.18
